TPU v7x, 256 devices: a 2x2x32 block of a 4x8x32 slice. The times are simulated.
256 devices in a mesh: grp: 4 (over y, x), ep: 64 (over z, core).
Axes of the slice: x: 2, y: 2, z: 32, core: 2. Of those that a mesh axis runs over, the one named last changes fastest.
The devices are a block of a 4x8x32 slice.
Arguments:
- tokens: bfloat16 [2048, 2048], P(('grp', 'ep')), parts along dimension 0, may hold values from -6 to 6
- routes: int32 [2048, 4], P(('grp', 'ep')), parts along dimension 0, may hold values from 0 to 63, all different within a row; in each aligned block of 8 rows (0 to 7, 8 to 15, ...) at most 2 rows name the same one
- gate_weights: float32 [2048, 4], P(('grp', 'ep')), parts along dimension 0, may hold values from 0.1 to 1
- norm_gain: float32 [2048], replicated, may hold values from 0.1 to 1.9
- final_gain: float32 [2048], replicated, may hold values from 0.1 to 1.9
- w_gate: bfloat16 [64, 2048, 512], P('ep'), may hold values from -0.088388348 to 0.088388348
- w_up: bfloat16 [64, 2048, 512], P('ep'), may hold values from -0.088388348 to 0.088388348
- w_down: bfloat16 [64, 512, 2048], P('ep'), may hold values from -0.176776695 to 0.176776695
Outputs:
- mixed: bfloat16 [2048, 2048], P('grp', 'ep'), parts along dimension 0
There are 4 independent parts, one for each index of `grp`. A program takes and returns all parts, laid end to end along the dimension named above; an argument that names none is the same for every part. Nothing has to cross between parts.
Inputs may be any that keep to these rules, and one draw needn't show every extreme that they name: `routes`: each row names 4 different experts; among the rows of one device no expert is named by more than 2 rows, and some expert reaches 2.
All inputs are finite; a program needn't handle non-finite values.
Results may differ from a plain program's by a relative error of at most 0.008.
Values may be sent and summed in bfloat16 or wider, within the bound.
No kernel may reach another device: no remote copies, remote signals or barrier semaphores. Data moves between devices by JAX's collectives and lax.ppermute only.
A program may use at most 64 MiB of HBM per device.

v0:
```python
import functools

import jax
import jax.numpy as jnp
from jax import lax
from jax.experimental import pallas as pl
from jax.experimental.pallas import tpu as pltpu
from jax.sharding import Mesh
from jax.sharding import PartitionSpec as P

EP = ("zh", "zl", "core")
CHIPS = ("zh", "zl")
GRP_EP = ("grp", "zh", "zl", "core")
LANES = 128
CLASSES = 4
EPSILON = 1e-06
F32 = jnp.float32
BF16 = jnp.bfloat16

VMEM = pl.BlockSpec(memory_space=pltpu.VMEM)
SMEM = pl.BlockSpec(memory_space=pltpu.SMEM)
HBM = pl.BlockSpec(memory_space=pltpu.HBM)


def by_class(parts, is_core, is_odd):
    a, b, c, d = parts
    a, b, c, d = (
        jnp.where(is_core, b, a),
        jnp.where(is_core, a, b),
        jnp.where(is_core, d, c),
        jnp.where(is_core, c, d),
    )
    return (
        jnp.where(is_odd, c, a),
        jnp.where(is_odd, d, b),
        jnp.where(is_odd, a, c),
        jnp.where(is_odd, b, d),
    )


def payload_kernel(tokens_ref, routes_ref, gates_ref, gain_ref, out_ref, meta_ref):
    width = tokens_ref.shape[1]
    per_dev = tokens_ref.shape[0]
    topk = routes_ref.shape[0]
    values = tokens_ref[...].astype(F32)
    mean = jnp.mean(values * values, axis=1, keepdims=True)
    out_ref[:, :width] = (values * lax.rsqrt(mean + EPSILON) * gain_ref[...]).astype(BF16)
    gates = gates_ref[...]
    high = gates.astype(BF16).astype(F32)
    mid = (gates - high).astype(BF16).astype(F32)
    meta_ref[...] = jnp.zeros(meta_ref.shape, F32)
    meta_ref[0:topk, 0:per_dev] = routes_ref[...].astype(F32)
    meta_ref[topk : 2 * topk, 0:per_dev] = high
    meta_ref[2 * topk : 3 * topk, 0:per_dev] = mid
    meta_ref[3 * topk : 4 * topk, 0:per_dev] = gates - high - mid
    out_ref[:, width:] = jnp.transpose(meta_ref[...])[:per_dev, :].astype(BF16)


def shed(load, capacity):
    group = load.shape[0]
    even = lax.broadcasted_iota(jnp.int32, load.shape, 0) % 2 == 0
    at = lambda x, d: pltpu.roll(x, (-d) % group, 0)
    chip = load + jnp.where(even, at(load, 1), at(load, -1))
    half = capacity // 2
    over = jnp.where(chip > capacity, jnp.maximum(load - half, 0.0), 0.0)
    kept = load - over
    settled = jnp.where(even, kept + at(kept, 1) + at(over, -2) + at(over, 3), 0.0)
    return kept, chip, settled


def windows(at_ref, keep_ref, got_ref):
    is_core = at_ref[1] == 1
    chips, cols, slots = keep_ref.shape
    keep = keep_ref[...].astype(F32).reshape(chips * cols, slots)
    got = got_ref[...].astype(F32).reshape(chips * cols, slots)
    return jnp.where(is_core, got, keep), jnp.where(is_core, keep, got)


def spill_kernel(at_ref, keep_ref, got_ref, right_ref, left_ref):
    low, high = windows(at_ref, keep_ref, got_ref)
    rows = right_ref.shape[0]
    side = LANES // 2
    lane = lax.broadcasted_iota(jnp.int32, (rows, LANES), 1)
    right_ref[...] = jnp.where(
        lane >= side, low[:rows], pltpu.roll(low[rows:], side, 1)
    ).astype(BF16)
    left_ref[...] = jnp.where(
        lane < side, high[:rows], pltpu.roll(high[rows:], side, 1)
    ).astype(BF16)


def pooled_pack_kernel(capacity, at_ref, keep_ref, got_ref, right_ref, left_ref, load_ref, out_ref):
    low, high = windows(at_ref, keep_ref, got_ref)
    chips, cols, slots = keep_ref.shape
    extra = capacity - slots
    half = capacity // 2
    load = load_ref[...]
    group = load.shape[0]
    kept, _, _ = shed(load, capacity)
    over = load - kept
    row = lax.broadcasted_iota(jnp.int32, load.shape, 0)
    first = at_ref[0] // 2 * 2
    one = lambda x, e: jnp.max(jnp.where(row == (e + group) % group, x, 0.0)).astype(jnp.int32)
    kept_low, kept_high = one(kept, first), one(kept, first + 1)
    from_left, from_right = one(over, first - 2), one(over, first + 3)
    lane = lax.broadcasted_iota(jnp.int32, low.shape, 1)
    side = LANES // 2
    unfold = lambda ref: jnp.concatenate(
        [ref[...].astype(F32), pltpu.roll(ref[...].astype(F32), side, 1)], axis=0
    )
    low = jnp.where(lane < kept_low, low, 0.0)
    high = jnp.where(lane >= slots - kept_high, high, 0.0)
    left = unfold(right_ref)
    left = jnp.where((lane >= half) & (lane < half + from_left), left, 0.0)
    right = unfold(left_ref)
    top = slots - 1 - half
    right = jnp.where((lane <= top) & (lane > top - from_right), right, 0.0)
    high = pltpu.roll(high, extra, 1)
    left = pltpu.roll(left, (kept_low - half + slots) % slots, 1)
    right = pltpu.roll(right, (capacity - 1 - kept_high - top + slots) % slots, 1)
    main = low + jnp.where(lane >= extra, high, 0.0)
    main = main + jnp.where(lane >= kept_low, left, 0.0)
    main = main + jnp.where(lane >= extra - kept_high, right, 0.0)
    tail = jnp.where(lane < extra, high, 0.0)
    tail = tail + jnp.where(lane < kept_low, left, 0.0)
    tail = tail + jnp.where(lane < extra - kept_high, right, 0.0)
    store_packed(main, tail, extra, out_ref)


def store_packed(main, tail, extra, out_ref):
    chips, packed, slots = out_ref.shape
    cols = main.shape[0] // chips
    groups = slots // extra
    each = cols // groups
    out_ref[:, :cols, :] = main.reshape(chips, cols, slots).astype(BF16)
    tail = tail.reshape(chips, cols, slots)
    out = tail[:, :each].reshape(chips * each, slots)
    for g in range(1, groups):
        out = out + pltpu.roll(
            tail[:, g * each : (g + 1) * each].reshape(chips * each, slots), g * extra, 1
        )
    out_ref[:, cols:, :] = out.reshape(chips, each, slots).astype(BF16)


def experts_kernel(
    topk, sizes, at_ref, a_ref, b_ref, c_ref, d_ref, wg_hbm, wu_hbm, wd_hbm,
    rank_ref, keep_ref, send_ref, load_ref, level_ref, wg_ref, wu_ref, wd_ref, sems,
):
    copies = [
        pltpu.make_async_copy(src.at[0], dst, sems.at[i])
        for i, (src, dst) in enumerate(((wg_hbm, wg_ref), (wu_hbm, wu_ref), (wd_hbm, wd_ref)))
    ]
    for copy in copies:
        copy.start()
    width = wg_ref.shape[0]
    is_core = at_ref[1] == 1
    is_odd = at_ref[2] == 1
    me = at_ref[0].astype(F32)
    group, total = rank_ref.shape
    chips, cols, slots = keep_ref.shape
    per_dev = total // group
    part = a_ref.shape[0]
    outer = part // per_dev
    refs = (a_ref, b_ref, c_ref, d_ref)
    meta = by_class([r[:, width:].astype(F32) for r in refs], is_core, is_odd)
    grouped = jnp.concatenate([jnp.transpose(m) for m in meta], axis=1)
    rows = jnp.concatenate(
        [m[i * per_dev : (i + 1) * per_dev] for i in range(outer) for m in meta], axis=0
    )
    ordered = jnp.concatenate(
        [jnp.transpose(rows[i * LANES : (i + 1) * LANES]) for i in range(total // LANES)], axis=1
    )
    expert = lax.broadcasted_iota(jnp.int32, (group, total), 0).astype(F32)
    match = jnp.zeros((group, total), F32)
    for k in range(topk):
        match = match + jnp.where(ordered[k : k + 1, :] == expert, 1.0, 0.0)
    index = lax.broadcasted_iota(jnp.int32, (total, total), 0)
    at = lax.broadcasted_iota(jnp.int32, (total, total), 1)
    place = at % part // per_dev * (per_dev * CLASSES) + at // part * per_dev + at % per_dev
    counts = match.astype(BF16)
    rank = jnp.dot(
        counts, jnp.where(index < at, 1.0, 0.0).astype(BF16), preferred_element_type=F32
    )
    rank_ref[...] = jnp.where(match > 0.0, rank, -1.0)
    moved = jnp.dot(
        counts, jnp.where(index < place, 1.0, 0.0).astype(BF16), preferred_element_type=F32
    )
    slot = jnp.sum(jnp.where(expert == me, moved, 0.0), axis=0, keepdims=True)
    slot = jnp.where(is_core, slots - 1 - slot, slot)
    gates = grouped[topk : 2 * topk] + grouped[2 * topk : 3 * topk] + grouped[3 * topk : 4 * topk]
    mine = jnp.zeros((1, total), F32)
    gate = jnp.zeros((1, total), F32)
    for k in range(topk):
        named = grouped[k : k + 1, :] == me
        mine = jnp.where(named, 1.0, mine)
        gate = jnp.where(named, gates[k : k + 1, :], gate)
    slot = jnp.where(mine > 0.0, slot, -1.0).astype(jnp.int32)
    gate = jnp.concatenate(
        by_class([gate[:, k * part : (k + 1) * part] for k in range(CLASSES)], is_core, is_odd), axis=1
    )
    slot = jnp.concatenate(
        by_class([slot[:, k * part : (k + 1) * part] for k in range(CLASSES)], is_core, is_odd), axis=1
    )
    load = jnp.broadcast_to(jnp.sum(match, axis=1, keepdims=True), (group, LANES))
    load_ref[...] = load
    kept, chip, settled = shed(load, sizes[0])
    most = jnp.max(chip).astype(jnp.int32)
    fits = (jnp.max(settled).astype(jnp.int32) <= sizes[0]).astype(jnp.int32)
    level_ref[0] = jnp.where(
        most <= sizes[0], 0, jnp.where(most <= sizes[1], 1, 3 - fits)
    ).astype(jnp.int32)

    hit = lax.broadcasted_iota(jnp.int32, (slots, total), 0) == slot
    pick = jnp.where(hit, 1.0, 0.0).astype(BF16)
    gate = jnp.sum(jnp.where(hit, gate, 0.0), axis=1, keepdims=True)
    picked = jnp.zeros((slots, width), F32)
    for k, ref in enumerate(refs):
        picked = picked + jnp.dot(
            pick[:, k * part : (k + 1) * part], ref[:, :width], preferred_element_type=F32
        )
    picked = picked.astype(BF16)
    copies[0].wait()
    gate_val = jnp.dot(picked, wg_ref[...], preferred_element_type=F32)
    copies[1].wait()
    up_val = jnp.dot(picked, wu_ref[...], preferred_element_type=F32)
    act = (gate_val * jax.nn.sigmoid(gate_val) * up_val * gate).astype(BF16)
    copies[2].wait()
    result = jnp.dot(act, wd_ref[...], preferred_element_type=F32)
    result = jnp.transpose(result).reshape(chips, 2, cols, slots)
    even, odd = result[:, 0], result[:, 1]
    keep_ref[...] = jnp.where(is_core, odd, even).astype(BF16)
    send_ref[...] = jnp.where(is_core, even, odd).astype(BF16)


def pack_kernel(capacity, at_ref, keep_ref, got_ref, out_ref):
    low, high = windows(at_ref, keep_ref, got_ref)
    extra = capacity - keep_ref.shape[2]
    if extra == keep_ref.shape[2]:
        main, tail = low, high
    else:
        high = pltpu.roll(high, extra, 1)
        spill = lax.broadcasted_iota(jnp.int32, high.shape, 1) < extra
        main = low + jnp.where(spill, 0.0, high)
        tail = jnp.where(spill, high, 0.0)
    store_packed(main, tail, extra, out_ref)


def combine_kernel(capacity, pooled, rows_ref, rank_ref, load_ref, out_ref, square_ref, kept_ref):
    cols, total = out_ref.shape
    chips = rows_ref.shape[0]
    extra = capacity - LANES
    groups = LANES // extra
    each = cols // groups
    row = lax.broadcasted_iota(jnp.int32, (2 * LANES, total), 0)
    slot = jnp.where(row < LANES, row, LANES + (row - LANES) % extra).astype(F32).astype(BF16)
    col = lax.broadcasted_iota(jnp.int32, (cols, LANES), 0)
    lane = lax.broadcasted_iota(jnp.int32, (cols, LANES), 1)
    own = (col // each) == (lane // extra)
    one = jnp.ones((), BF16)
    zero = jnp.zeros((), BF16)
    group = rank_ref.shape[0]
    half = capacity // 2
    if pooled:
        kept, _, _ = shed(load_ref[...], capacity)
        kept_ref[...] = jnp.concatenate([kept] * (total // LANES), axis=1)

    def step(s, acc):
        low = rank_ref[pl.ds(2 * s, 1), :]
        high = rank_ref[pl.ds(2 * s + 1, 1), :]
        if pooled:
            kept_low = kept_ref[pl.ds(2 * s, 1), :]
            kept_high = kept_ref[pl.ds(2 * s + 1, 1), :]
            before = lax.rem(2 * s - 2 + group, group)
            after = lax.rem(2 * s + 3, group)
            left = rank_ref[pl.ds(before, 1), :]
            right = rank_ref[pl.ds(after, 1), :]
            left = jnp.where(left < kept_ref[pl.ds(before, 1), :], -1.0, kept_low + left - half)
            right = jnp.where(
                right < kept_ref[pl.ds(after, 1), :],
                -1.0,
                capacity - 1.0 - (kept_high + right - half),
            )
            low = jnp.where(low < kept_low, low, -1.0)
            high = jnp.where(high < kept_high, high, -1.0)
        high = jnp.where(high < 0.0, -1.0, capacity - 1.0 - high)
        hit = (slot == low.astype(BF16)) | (slot == high.astype(BF16))
        if pooled:
            hit = hit | (slot == left.astype(BF16)) | (slot == right.astype(BF16))
        pick = jnp.where(hit, one, zero)
        block = rows_ref[s].astype(F32)
        tail = jnp.concatenate([block[cols:]] * groups, axis=0)
        tail = jnp.where(own, tail, 0.0)
        left = jnp.concatenate([block[:cols], tail], axis=1).astype(BF16)
        return acc + jnp.dot(left, pick, preferred_element_type=F32)

    out = lax.fori_loop(0, chips, step, jnp.zeros((cols, total), F32), unroll=4)
    out_ref[...] = out
    square_ref[...] = jnp.sum(out * out, axis=0, keepdims=True)


def spread_kernel(mine_ref, other_ref, out_ref):
    square = mine_ref[...] + other_ref[...]
    chips, lines, _ = out_ref.shape
    for i in range(lines):
        out_ref[:, i : i + 1, :] = jnp.broadcast_to(
            square[None, :, i * LANES : (i + 1) * LANES], (chips, 1, LANES)
        ).astype(BF16)


def finish_kernel(width, at_ref, squares_ref, mixed_ref, gain_ref, out_ref):
    sums = jnp.sum(squares_ref[...].astype(F32), axis=0)
    mean = jnp.concatenate([sums[i : i + 1] for i in range(sums.shape[0])], axis=1) / width
    cols = mixed_ref.shape[0]
    each = LANES // cols
    me = at_ref[0]
    gain = jnp.broadcast_to(gain_ref[pl.ds(me // each, 1), :], (LANES, LANES))
    gain = pltpu.roll(gain, (each - me % each) % each * cols, 1)
    gain = jnp.transpose(gain)[:cols, :1]
    out_ref[...] = (mixed_ref[...] * lax.rsqrt(mean + EPSILON) * gain).astype(BF16)


def shards(tokens, routes, gate_weights, norm_gain, final_gain, w_gate, w_up, w_down):
    per_dev, width = tokens.shape
    topk = routes.shape[1]
    group = lax.axis_size(EP)
    chips = group // 2
    cols = width // group
    total = per_dev * group
    most = 2 * group
    me = lax.axis_index(EP)
    core = lax.axis_index("core")
    odd = lax.axis_index("zl")
    at = jnp.stack([me, core, odd]).astype(jnp.int32)

    payload = pl.pallas_call(
        payload_kernel,
        out_shape=jax.ShapeDtypeStruct((per_dev, width + LANES), BF16),
        scratch_shapes=[pltpu.VMEM((LANES, LANES), F32)],
    )(tokens, jnp.transpose(routes), jnp.transpose(gate_weights), norm_gain[None, :])

    zigzag = []
    for chip in range(chips):
        zigzag.append((chip * 2, ((chip + 1) % chips) * 2))
        zigzag.append((chip * 2 + 1, ((chip - 1) % chips) * 2 + 1))
    swap = [(0, 1), (1, 0)]
    own = lax.all_gather(payload, "zh", axis=0, tiled=True)
    near = lax.ppermute(own, EP, zigzag)
    own_pair = lax.ppermute(own, "core", swap)
    near_pair = lax.ppermute(near, "core", swap)
    pieces = (own, own_pair, near, near_pair)
    part = own.shape[0]

    window = jax.ShapeDtypeStruct((chips, cols, LANES), BF16)
    sizes = (most * 5 // 4, most * 3 // 2, most * 2)
    rank, keep, send, load, level = pl.pallas_call(
        functools.partial(experts_kernel, topk, sizes),
        in_specs=[SMEM] + [VMEM] * CLASSES + [HBM] * 3,
        out_specs=[VMEM, VMEM, VMEM, VMEM, SMEM],
        out_shape=[
            jax.ShapeDtypeStruct((group, total), F32),
            window,
            window,
            jax.ShapeDtypeStruct((group, LANES), F32),
            jax.ShapeDtypeStruct((1,), jnp.int32),
        ],
        scratch_shapes=[
            pltpu.VMEM(w_gate.shape[1:], BF16),
            pltpu.VMEM(w_up.shape[1:], BF16),
            pltpu.VMEM(w_down.shape[1:], BF16),
            pltpu.SemaphoreType.DMA((3,)),
        ],
        compiler_params=pltpu.CompilerParams(vmem_limit_bytes=50 << 20),
    )(at, *pieces, w_gate, w_up, w_down)
    got = lax.ppermute(send, "core", swap)
    lines = total // LANES

    right = [(i, (i + 2) % group) for i in range(group)]
    left = [(i, (i - 2) % group) for i in range(group)]
    small = pltpu.CompilerParams(vmem_limit_bytes=16 << 20)

    def branch(capacity, pooled):
        packed = cols * capacity // LANES
        message = jax.ShapeDtypeStruct((chips, packed, LANES), BF16)
        spill = jax.ShapeDtypeStruct((chips * cols // 2, LANES), BF16)

        def run(at, keep, got, rank, load):
            if pooled:
                to_right, to_left = pl.pallas_call(
                    spill_kernel,
                    in_specs=[SMEM, VMEM, VMEM],
                    out_shape=[spill, spill],
                    compiler_params=small,
                )(at, keep, got)
                both = pl.pallas_call(
                    functools.partial(pooled_pack_kernel, capacity),
                    in_specs=[SMEM] + [VMEM] * 5,
                    out_shape=message,
                    compiler_params=small,
                )(at, keep, got, lax.ppermute(to_right, EP, right), lax.ppermute(to_left, EP, left), load)
            else:
                both = pl.pallas_call(
                    functools.partial(pack_kernel, capacity),
                    in_specs=[SMEM, VMEM, VMEM],
                    out_shape=message,
                    compiler_params=small,
                )(at, keep, got)
            returned = lax.all_to_all(both, CHIPS, split_axis=0, concat_axis=0, tiled=True)
            return pl.pallas_call(
                functools.partial(combine_kernel, capacity, pooled),
                in_specs=[VMEM] * 3,
                out_shape=[
                    jax.ShapeDtypeStruct((cols, total), F32),
                    jax.ShapeDtypeStruct((1, total), F32),
                ],
                scratch_shapes=[pltpu.VMEM((group, total), F32)],
                compiler_params=small,
            )(returned, rank, load)

        return run

    mixed, square = lax.switch(
        level[0],
        [branch(sizes[0], False), branch(sizes[1], False), branch(sizes[0], True), branch(sizes[2], False)],
        at, keep, got, rank, load,
    )

    spread = pl.pallas_call(
        spread_kernel,
        in_specs=[VMEM] * 2,
        out_shape=jax.ShapeDtypeStruct((chips, total // LANES, LANES), BF16),
        compiler_params=small,
    )(square, lax.ppermute(square, "core", swap))
    squares = lax.all_to_all(spread, CHIPS, split_axis=0, concat_axis=0, tiled=True)
    finished = pl.pallas_call(
        functools.partial(finish_kernel, width),
        in_specs=[SMEM] + [VMEM] * 3,
        out_shape=jax.ShapeDtypeStruct((cols, total), BF16),
        compiler_params=small,
    )(at, squares, mixed, final_gain.reshape(-1, LANES))
    return jnp.transpose(finished)


def solution(mesh):
    split = Mesh(mesh.devices.reshape(mesh.shape["grp"], 16, 2, 2), GRP_EP)
    return jax.shard_map(
        shards,
        mesh=split,
        in_specs=(
            P(GRP_EP, None),
            P(GRP_EP, None),
            P(GRP_EP, None),
            P(),
            P(),
            P(EP, None, None),
            P(EP, None, None),
            P(EP, None, None),
        ),
        out_specs=P("grp", EP),
        check_vma=False,
    )
```

profile of v0, /device:TPU:46, one launch (start us, length us, event | category | flops | bytes accessed | tf_op | source)
XLA Modules:
  0.0 175.0 jit_solution(585604220541672425)
XLA Ops:
  0.0 1.5 shard_map.82
  1.5 56.7 %all_gather.3.a_ref = bf16[128,2176]{1,0:T(8,128)(2,1)S(1)} all-gather(bf16[8,2176]{1,0:T(8,128)(2,1)} %shard_map.82), channel_id=1, replica_groups=mesh['grp'=4,'zh'=16,'zl'=2,'core'=2] {'zh'}, dimensions={0}, use_global_device_ids=true | all-gather | bytes 591872 | tf_op jit(solution)/shard_map/all_gather | solution.py:346
  58.2 2.9 %collective-permute-start.3 = (bf16[128,2176]{1,0:T(8,128)(2,1)S(1)}, bf16[128,2176]{1,0:T(8,128)(2,1)S(1)}, u32[]{:S(2)}, u32[]{:S(2)}) collective-permute-start(bf16[128,2176]{1,0:T(8,128)(2,1)S(1)} %all_gather.3.a_ref), channel_id=1, source_target_pairs={{0,2},{1,63},{2,4},{3,1},{4,6},{5,3},{6,8},{7,5},{8,10},{9,7},{10,... | collective-permute-start | bytes 1671176 | tf_op jit(solution)/shard_map/ppermute | solution.py:347
  61.1 0.0 collective-permute-start.2
  61.1 7.9 %collective-permute-done.3.c_ref = bf16[128,2176]{1,0:T(8,128)(2,1)S(1)} collective-permute-done((bf16[128,2176]{1,0:T(8,128)(2,1)S(1)}, bf16[128,2176]{1,0:T(8,128)(2,1)S(1)}, u32[]{:S(2)}, u32[]{:S(2)}) %collective-permute-start.3) | collective-permute-done | bytes 557088 | tf_op jit(solution)/shard_map/ppermute | solution.py:347
  68.9 0.0 collective-permute-start.4
  68.9 0.1 pad_add_fusion.at_ref
  69.0 0.0 collective-permute-done.2.b_ref
  69.0 1.9 %collective-permute-done.4.d_ref = bf16[128,2176]{1,0:T(8,128)(2,1)S(1)} collective-permute-done((bf16[128,2176]{1,0:T(8,128)(2,1)S(1)}, bf16[128,2176]{1,0:T(8,128)(2,1)S(1)}, u32[]{:S(2)}, u32[]{:S(2)}) %collective-permute-start.4) | collective-permute-done | bytes 557088 | tf_op jit(solution)/shard_map/ppermute | solution.py:349
  70.9 4.9 %shard_map.83 = (f32[64,512]{1,0:T(8,128)S(1)}, bf16[32,32,128]{2,1,0:T(8,128)(2,1)S(1)}, bf16[32,32,128]{2,1,0:T(8,128)(2,1)S(1)}, f32[64,128]{1,0:T(8,128)S(1)}, s32[1]{0:T(128)}) custom-call(s32[3]{0:T(128)S(1)} %pad_add_fusion.at_ref, bf16[128,2176]{1,0:T(8,128)(2,1)S(1)} %all_gather.3.a_ref, bf16[128,2176]{1,0:T(8,128)(2,1)S(1)} %collective-permute-done.2.b_ref, ...), custom_call_target="tpu_custom_call" | custom-call | tf_op jit(solution)/shard_map/pallas_call | solution.py:355
  75.8 0.3 collective-permute-start.5
  76.7 0.7 collective-permute-done.5
  77.5 0.0 copy-start
  77.5 68.0 %conditional.1 = ((f32[32,512]{1,0:T(8,128)S(1)}, f32[1,512]{1,0:T(1,128)S(1)})) conditional(s32[]{:T(128)} %bitcast.6, (s32[3]{0:T(128)S(1)}, bf16[32,32,128]{2,1,0:T(8,128)(2,1)S(1)}, bf16[32,32,128]{2,1,0:T(8,128)(2,1)S(1)}, f32[64,512]{1,0:T(8,128)S(1)}, f32[64,128]{1,0:T(8,128)S(1)}) %tuple.17, (s32[3]{0:T(128)S(1)}, ...), branch_computations={%region_0.0_spmd, %region_1.0_spmd, %region_2.0_spmd, %region_3.0_... | conditional | bytes 1704024 | solution.py:421
  77.5 0.8 branch_1_fun.2
  78.3 64.7 %all_to_all.22.rows_ref = bf16[32,48,128]{2,1,0:T(8,128)(2,1)S(1)} all-to-all(bf16[32,48,128]{2,1,0:T(8,128)(2,1)S(1)} %branch_1_fun.2), channel_id=1, replica_groups=mesh['grp'=4,'zh'=16,'zl'=2,'core'=2] {'zh','zl'}, dimensions={0} | all-to-all | bytes 786432 | tf_op jit(solution)/shard_map/cond/branch_1_fun/all_to_all | solution.py:407
  143.0 2.5 %branch_1_fun.3 = (f32[32,512]{1,0:T(8,128)S(1)}, f32[1,512]{1,0:T(1,128)S(1)}) custom-call(bf16[32,48,128]{2,1,0:T(8,128)(2,1)S(1)} %all_to_all.22.rows_ref, f32[64,512]{1,0:T(8,128)S(1)} %get-tuple-element.53.rank_ref, f32[64,128]{1,0:T(8,128)S(1)} %get-tuple-element.54.load_ref), custom_call_target="tpu_custom_call" | custom-call | tf_op jit(solution)/shard_map/cond/branch_1_fun/pallas_call | solution.py:408
  145.5 0.1 collective-permute-start.6
  145.6 1.1 collective-permute-done.6.other_ref
  146.8 26.8 %all_to_all.25.squares_ref = bf16[32,4,128]{2,1,0:T(4,128)(2,1)S(1)} all-to-all(bf16[32,4,128]{2,1,0:T(4,128)(2,1)S(1)} %shard_map.84), channel_id=1, replica_groups=mesh['grp'=4,'zh'=16,'zl'=2,'core'=2] {'zh','zl'}, dimensions={0} | all-to-all | bytes 65536 | tf_op jit(solution)/shard_map/all_to_all | solution.py:433
  173.6 0.0 copy-done
  173.6 1.4 shard_map.85
  (1 shorter events, 0.0 us)
Async XLA Ops:
  58.2 10.7 %collective-permute-start.3 = (bf16[128,2176]{1,0:T(8,128)(2,1)S(1)}, bf16[128,2176]{1,0:T(8,128)(2,1)S(1)}, u32[]{:S(2)}, u32[]{:S(2)}) collective-permute-start(bf16[128,2176]{1,0:T(8,128)(2,1)S(1)} %all_gather.3.a_ref), channel_id=1, source_target_pairs={{0,2},{1,63},{2,4},{3,1},{4,6},{5,3},{6,8},{7,5},{8,10},{9,7},{10,... | collective-permute-start | bytes 1671176 | tf_op jit(solution)/shard_map/ppermute | solution.py:347
  61.1 8.0 %collective-permute-start.2 = (bf16[128,2176]{1,0:T(8,128)(2,1)S(1)}, bf16[128,2176]{1,0:T(8,128)(2,1)S(1)}, u32[]{:S(2)}, u32[]{:S(2)}) collective-permute-start(bf16[128,2176]{1,0:T(8,128)(2,1)S(1)} %all_gather.3.a_ref), channel_id=1, source_target_pairs={{0,1},{1,0},{2,3},{3,2},{4,5},{5,4},{6,7},{7,6},{8,9},{9,8},{10,11... | collective-permute-start | bytes 1671176 | tf_op jit(solution)/shard_map/ppermute | solution.py:348
  68.9 2.0 %collective-permute-start.4 = (bf16[128,2176]{1,0:T(8,128)(2,1)S(1)}, bf16[128,2176]{1,0:T(8,128)(2,1)S(1)}, u32[]{:S(2)}, u32[]{:S(2)}) collective-permute-start(bf16[128,2176]{1,0:T(8,128)(2,1)S(1)} %collective-permute-done.3.c_ref), channel_id=1, source_target_pairs={{0,1},{1,0},{2,3},{3,2},{4,5},{5,4},{6,7},{7,6},{8,9},{9,8},{10,11... | collective-permute-start | bytes 1671176 | tf_op jit(solution)/shard_map/ppermute | solution.py:349
  75.8 1.7 collective-permute-start.5
  77.5 96.1 %copy-start = (f32[2048]{0:T(1024)S(1)}, f32[2048]{0:T(1024)}, u32[]{:S(2)}) copy-start(f32[2048]{0:T(1024)} %param.16) | copy-start | bytes 24580
  145.5 1.3 collective-permute-start.6
where the time goes:
time: 173 us; the launch traced here: 175 us
  blocking collectives  148 us (86%)
  waiting for transfers between devices  11.6 us (7%)
  Pallas kernels  11.1 us (6%)
  starting transfers between devices  3.27 us (2%)
    all_to_all x1, blocking collectives, run(): lax.all_to_all(both, CHIPS, split_axis=0, concat_axis=0, tiled=True)  64.7 us
    all_gather x1, blocking collectives, shards(): own = lax.all_gather(payload, 'zh', axis=0, tiled=True)  56.7 us
    all_to_all x1, blocking collectives, shards(): lax.all_to_all(spread, CHIPS, split_axis=0, concat_axis=0, tiled=True)  26.8 us
    ppermute x1, waiting for transfers between devices, shards(): near = lax.ppermute(own, EP, zigzag)  7.88 us
    pallas_call x1, Pallas kernels, shards(): pl.pallas_call(functools.partial(experts_kernel, topk, sizes), in_specs=[...  4.9 us
  transfers between devices with their start and end apart: 5, of which 4 were waited for; matrix products, arithmetic and copies ran while one was open for 0% of the time, Pallas kernels for 0%

commit v1 on v0

--- a/solution.py
+++ b/solution.py
@@ -89,7 +89,7 @@
     ).astype(BF16)
 
 
-def pooled_pack_kernel(capacity, at_ref, keep_ref, got_ref, right_ref, left_ref, load_ref, out_ref):
+def pooled_pack_kernel(capacity, at_ref, keep_ref, got_ref, right_ref, left_ref, load_ref, out_ref, took_ref):
     low, high = windows(at_ref, keep_ref, got_ref)
     chips, cols, slots = keep_ref.shape
     extra = capacity - slots
@@ -100,6 +100,11 @@
     over = load - kept
     row = lax.broadcasted_iota(jnp.int32, load.shape, 0)
     first = at_ref[0] // 2 * 2
+    came = pltpu.roll(over, 2, 0) + pltpu.roll(over, group - 3, 0)
+    bit = jnp.where((row % 2 == 0) & (came > 0.0), jnp.left_shift(1, row % 32 // 2), 0)
+    halves = [jnp.where(row // 32 == h, bit, 0) for h in range(group // 32)]
+    for h, half_bits in enumerate(halves):
+        took_ref[h] = jnp.max(jnp.sum(half_bits, axis=0, keepdims=True).astype(F32)).astype(jnp.int32)
     one = lambda x, e: jnp.max(jnp.where(row == (e + group) % group, x, 0.0)).astype(jnp.int32)
     kept_low, kept_high = one(kept, first), one(kept, first + 1)
     from_left, from_right = one(over, first - 2), one(over, first + 3)
@@ -150,8 +155,8 @@
         pltpu.make_async_copy(src.at[0], dst, sems.at[i])
         for i, (src, dst) in enumerate(((wg_hbm, wg_ref), (wu_hbm, wu_ref), (wd_hbm, wd_ref)))
     ]
-    for copy in copies:
-        copy.start()
+    copies[0].start()
+    copies[1].start()
     width = wg_ref.shape[0]
     is_core = at_ref[1] == 1
     is_odd = at_ref[2] == 1
@@ -220,6 +225,7 @@
         )
     picked = picked.astype(BF16)
     copies[0].wait()
+    copies[2].start()
     gate_val = jnp.dot(picked, wg_ref[...], preferred_element_type=F32)
     copies[1].wait()
     up_val = jnp.dot(picked, wu_ref[...], preferred_element_type=F32)
@@ -245,7 +251,7 @@
     store_packed(main, tail, extra, out_ref)
 
 
-def combine_kernel(capacity, pooled, rows_ref, rank_ref, load_ref, out_ref, square_ref, kept_ref):
+def combine_kernel(capacity, pooled, took_ref, rows_ref, rank_ref, load_ref, out_ref, square_ref, kept_ref):
     cols, total = out_ref.shape
     chips = rows_ref.shape[0]
     extra = capacity - LANES
@@ -264,28 +270,7 @@
         kept, _, _ = shed(load_ref[...], capacity)
         kept_ref[...] = jnp.concatenate([kept] * (total // LANES), axis=1)
 
-    def step(s, acc):
-        low = rank_ref[pl.ds(2 * s, 1), :]
-        high = rank_ref[pl.ds(2 * s + 1, 1), :]
-        if pooled:
-            kept_low = kept_ref[pl.ds(2 * s, 1), :]
-            kept_high = kept_ref[pl.ds(2 * s + 1, 1), :]
-            before = lax.rem(2 * s - 2 + group, group)
-            after = lax.rem(2 * s + 3, group)
-            left = rank_ref[pl.ds(before, 1), :]
-            right = rank_ref[pl.ds(after, 1), :]
-            left = jnp.where(left < kept_ref[pl.ds(before, 1), :], -1.0, kept_low + left - half)
-            right = jnp.where(
-                right < kept_ref[pl.ds(after, 1), :],
-                -1.0,
-                capacity - 1.0 - (kept_high + right - half),
-            )
-            low = jnp.where(low < kept_low, low, -1.0)
-            high = jnp.where(high < kept_high, high, -1.0)
-        high = jnp.where(high < 0.0, -1.0, capacity - 1.0 - high)
-        hit = (slot == low.astype(BF16)) | (slot == high.astype(BF16))
-        if pooled:
-            hit = hit | (slot == left.astype(BF16)) | (slot == right.astype(BF16))
+    def add(s, acc, hit):
         pick = jnp.where(hit, one, zero)
         block = rows_ref[s].astype(F32)
         tail = jnp.concatenate([block[cols:]] * groups, axis=0)
@@ -293,7 +278,43 @@
         left = jnp.concatenate([block[:cols], tail], axis=1).astype(BF16)
         return acc + jnp.dot(left, pick, preferred_element_type=F32)
 
-    out = lax.fori_loop(0, chips, step, jnp.zeros((cols, total), F32), unroll=4)
+    def keys(s):
+        low = rank_ref[pl.ds(2 * s, 1), :]
+        high = rank_ref[pl.ds(2 * s + 1, 1), :]
+        if pooled:
+            low = jnp.where(low < kept_ref[pl.ds(2 * s, 1), :], low, -1.0)
+            high = jnp.where(high < kept_ref[pl.ds(2 * s + 1, 1), :], high, -1.0)
+        high = jnp.where(high < 0.0, -1.0, capacity - 1.0 - high)
+        return (slot == low.astype(BF16)) | (slot == high.astype(BF16))
+
+    def step(s, acc):
+        return add(s, acc, keys(s))
+
+    out = lax.fori_loop(0, chips, step, jnp.zeros((cols, total), F32), unroll=8)
+    if pooled:
+
+        def more(s, acc):
+            def surplus(acc):
+                before = lax.rem(2 * s - 2 + group, group)
+                after = lax.rem(2 * s + 3, group)
+                left = rank_ref[pl.ds(before, 1), :]
+                right = rank_ref[pl.ds(after, 1), :]
+                left = jnp.where(
+                    left < kept_ref[pl.ds(before, 1), :],
+                    -1.0,
+                    kept_ref[pl.ds(2 * s, 1), :] + left - half,
+                )
+                right = jnp.where(
+                    right < kept_ref[pl.ds(after, 1), :],
+                    -1.0,
+                    capacity - 1.0 - (kept_ref[pl.ds(2 * s + 1, 1), :] + right - half),
+                )
+                return add(s, acc, (slot == left.astype(BF16)) | (slot == right.astype(BF16)))
+
+            took = (took_ref[s // 16] >> (s % 16)) & 1
+            return lax.cond(took == 1, surplus, lambda acc: acc, acc)
+
+        out = lax.fori_loop(0, chips, more, out)
     out_ref[...] = out
     square_ref[...] = jnp.sum(out * out, axis=0, keepdims=True)
 
@@ -391,13 +412,15 @@
                     out_shape=[spill, spill],
                     compiler_params=small,
                 )(at, keep, got)
-                both = pl.pallas_call(
+                both, took = pl.pallas_call(
                     functools.partial(pooled_pack_kernel, capacity),
                     in_specs=[SMEM] + [VMEM] * 5,
-                    out_shape=message,
+                    out_specs=[VMEM, SMEM],
+                    out_shape=[message, jax.ShapeDtypeStruct((group // 32,), jnp.int32)],
                     compiler_params=small,
                 )(at, keep, got, lax.ppermute(to_right, EP, right), lax.ppermute(to_left, EP, left), load)
             else:
+                took = at
                 both = pl.pallas_call(
                     functools.partial(pack_kernel, capacity),
                     in_specs=[SMEM, VMEM, VMEM],
@@ -407,14 +430,14 @@
             returned = lax.all_to_all(both, CHIPS, split_axis=0, concat_axis=0, tiled=True)
             return pl.pallas_call(
                 functools.partial(combine_kernel, capacity, pooled),
-                in_specs=[VMEM] * 3,
+                in_specs=[SMEM] + [VMEM] * 3,
                 out_shape=[
                     jax.ShapeDtypeStruct((cols, total), F32),
                     jax.ShapeDtypeStruct((1, total), F32),
                 ],
                 scratch_shapes=[pltpu.VMEM((group, total), F32)],
                 compiler_params=small,
-            )(returned, rank, load)
+            )(took, returned, rank, load)
 
         return run
 

time: 173 us -> 177 us (1.023); the launches traced: 175 us -> 176 us
  no operation moved by 1% of the time
where the time goes in v1:
time: 177 us; the launch traced here: 176 us
  blocking collectives  148 us (84%)
  Pallas kernels  11.6 us (7%)
  waiting for transfers between devices  11.6 us (7%)
  starting transfers between devices  3.27 us (2%)
    all_to_all x1, blocking collectives, run(): lax.all_to_all(both, CHIPS, split_axis=0, concat_axis=0, tiled=True)  64.7 us
    all_gather x1, blocking collectives, shards(): own = lax.all_gather(payload, 'zh', axis=0, tiled=True)  56.7 us
    all_to_all x1, blocking collectives, shards(): lax.all_to_all(spread, CHIPS, split_axis=0, concat_axis=0, tiled=True)  26.8 us
    ppermute x1, waiting for transfers between devices, shards(): near = lax.ppermute(own, EP, zigzag)  7.88 us
    pallas_call x1, Pallas kernels, shards(): pl.pallas_call(functools.partial(experts_kernel, topk, sizes), in_specs=[...  5.38 us
  transfers between devices with their start and end apart: 5, of which 4 were waited for; matrix products, arithmetic and copies ran while one was open for 0% of the time, Pallas kernels for 0%

profile of v1, /device:TPU:46, one launch (start us, length us, event | category | flops | bytes accessed | tf_op | source)
XLA Modules:
  0.0 175.5 jit_solution(12529975984627821896)
XLA Ops:
  0.0 1.5 shard_map.82
  1.5 56.7 %all_gather.3.a_ref = bf16[128,2176]{1,0:T(8,128)(2,1)S(1)} all-gather(bf16[8,2176]{1,0:T(8,128)(2,1)} %shard_map.82), channel_id=1, replica_groups=mesh['grp'=4,'zh'=16,'zl'=2,'core'=2] {'zh'}, dimensions={0}, use_global_device_ids=true | all-gather | bytes 591872 | tf_op jit(solution)/shard_map/all_gather | solution.py:367
  58.2 2.9 %collective-permute-start.3 = (bf16[128,2176]{1,0:T(8,128)(2,1)S(1)}, bf16[128,2176]{1,0:T(8,128)(2,1)S(1)}, u32[]{:S(2)}, u32[]{:S(2)}) collective-permute-start(bf16[128,2176]{1,0:T(8,128)(2,1)S(1)} %all_gather.3.a_ref), channel_id=1, source_target_pairs={{0,2},{1,63},{2,4},{3,1},{4,6},{5,3},{6,8},{7,5},{8,10},{9,7},{10,... | collective-permute-start | bytes 1671176 | tf_op jit(solution)/shard_map/ppermute | solution.py:368
  61.1 0.0 collective-permute-start.2
  61.1 7.9 %collective-permute-done.3.c_ref = bf16[128,2176]{1,0:T(8,128)(2,1)S(1)} collective-permute-done((bf16[128,2176]{1,0:T(8,128)(2,1)S(1)}, bf16[128,2176]{1,0:T(8,128)(2,1)S(1)}, u32[]{:S(2)}, u32[]{:S(2)}) %collective-permute-start.3) | collective-permute-done | bytes 557088 | tf_op jit(solution)/shard_map/ppermute | solution.py:368
  68.9 0.0 collective-permute-start.4
  69.0 0.1 pad_add_fusion.at_ref
  69.0 0.0 collective-permute-done.2.b_ref
  69.0 1.9 %collective-permute-done.4.d_ref = bf16[128,2176]{1,0:T(8,128)(2,1)S(1)} collective-permute-done((bf16[128,2176]{1,0:T(8,128)(2,1)S(1)}, bf16[128,2176]{1,0:T(8,128)(2,1)S(1)}, u32[]{:S(2)}, u32[]{:S(2)}) %collective-permute-start.4) | collective-permute-done | bytes 557088 | tf_op jit(solution)/shard_map/ppermute | solution.py:370
  70.9 5.4 %shard_map.83 = (f32[64,512]{1,0:T(8,128)S(1)}, bf16[32,32,128]{2,1,0:T(8,128)(2,1)S(1)}, bf16[32,32,128]{2,1,0:T(8,128)(2,1)S(1)}, f32[64,128]{1,0:T(8,128)S(1)}, s32[1]{0:T(128)}) custom-call(s32[3]{0:T(128)S(1)} %pad_add_fusion.at_ref, bf16[128,2176]{1,0:T(8,128)(2,1)S(1)} %all_gather.3.a_ref, bf16[128,2176]{1,0:T(8,128)(2,1)S(1)} %collective-permute-done.2.b_ref, ...), custom_call_target="tpu_custom_call" | custom-call | tf_op jit(solution)/shard_map/pallas_call | solution.py:376
  76.3 0.3 collective-permute-start.5
  77.2 0.7 collective-permute-done.5
  78.0 0.0 copy-start
  78.0 68.0 %conditional.1 = ((f32[32,512]{1,0:T(8,128)S(1)}, f32[1,512]{1,0:T(1,128)S(1)})) conditional(s32[]{:T(128)} %bitcast.6, (s32[3]{0:T(128)S(1)}, bf16[32,32,128]{2,1,0:T(8,128)(2,1)S(1)}, bf16[32,32,128]{2,1,0:T(8,128)(2,1)S(1)}, f32[64,512]{1,0:T(8,128)S(1)}, f32[64,128]{1,0:T(8,128)S(1)}) %tuple.17, (s32[3]{0:T(128)S(1)}, ...), branch_computations={%region_0.0_spmd, %region_1.0_spmd, %region_2.0_spmd, %region_3.0_... | conditional | bytes 1704024 | solution.py:444
  78.0 0.8 branch_1_fun.2
  78.8 64.7 %all_to_all.22.rows_ref = bf16[32,48,128]{2,1,0:T(8,128)(2,1)S(1)} all-to-all(bf16[32,48,128]{2,1,0:T(8,128)(2,1)S(1)} %branch_1_fun.2), channel_id=1, replica_groups=mesh['grp'=4,'zh'=16,'zl'=2,'core'=2] {'zh','zl'}, dimensions={0} | all-to-all | bytes 786432 | tf_op jit(solution)/shard_map/cond/branch_1_fun/all_to_all | solution.py:430
  143.5 2.5 %branch_1_fun.3 = (f32[32,512]{1,0:T(8,128)S(1)}, f32[1,512]{1,0:T(1,128)S(1)}) custom-call(s32[3]{0:T(128)S(1)} %get-tuple-element.50.at_ref.took_ref, bf16[32,48,128]{2,1,0:T(8,128)(2,1)S(1)} %all_to_all.22.rows_ref, f32[64,512]{1,0:T(8,128)S(1)} %get-tuple-element.53.rank_ref, f32[64,128]{1,0:T(8,128)S(1)} %get-tuple-element.54.load_ref), custom_call_target="tpu_custom_call" | custom-call | tf_op jit(solution)/shard_map/cond/branch_1_fun/pallas_call | solution.py:431
  146.0 0.1 collective-permute-start.6
  146.2 1.1 collective-permute-done.6.other_ref
  147.3 26.8 %all_to_all.25.squares_ref = bf16[32,4,128]{2,1,0:T(4,128)(2,1)S(1)} all-to-all(bf16[32,4,128]{2,1,0:T(4,128)(2,1)S(1)} %shard_map.84), channel_id=1, replica_groups=mesh['grp'=4,'zh'=16,'zl'=2,'core'=2] {'zh','zl'}, dimensions={0} | all-to-all | bytes 65536 | tf_op jit(solution)/shard_map/all_to_all | solution.py:456
  174.2 0.0 copy-done
  174.2 1.4 shard_map.85
  (1 shorter events, 0.0 us)
Async XLA Ops:
  58.2 10.7 %collective-permute-start.3 = (bf16[128,2176]{1,0:T(8,128)(2,1)S(1)}, bf16[128,2176]{1,0:T(8,128)(2,1)S(1)}, u32[]{:S(2)}, u32[]{:S(2)}) collective-permute-start(bf16[128,2176]{1,0:T(8,128)(2,1)S(1)} %all_gather.3.a_ref), channel_id=1, source_target_pairs={{0,2},{1,63},{2,4},{3,1},{4,6},{5,3},{6,8},{7,5},{8,10},{9,7},{10,... | collective-permute-start | bytes 1671176 | tf_op jit(solution)/shard_map/ppermute | solution.py:368
  61.1 8.0 %collective-permute-start.2 = (bf16[128,2176]{1,0:T(8,128)(2,1)S(1)}, bf16[128,2176]{1,0:T(8,128)(2,1)S(1)}, u32[]{:S(2)}, u32[]{:S(2)}) collective-permute-start(bf16[128,2176]{1,0:T(8,128)(2,1)S(1)} %all_gather.3.a_ref), channel_id=1, source_target_pairs={{0,1},{1,0},{2,3},{3,2},{4,5},{5,4},{6,7},{7,6},{8,9},{9,8},{10,11... | collective-permute-start | bytes 1671176 | tf_op jit(solution)/shard_map/ppermute | solution.py:369
  68.9 2.0 %collective-permute-start.4 = (bf16[128,2176]{1,0:T(8,128)(2,1)S(1)}, bf16[128,2176]{1,0:T(8,128)(2,1)S(1)}, u32[]{:S(2)}, u32[]{:S(2)}) collective-permute-start(bf16[128,2176]{1,0:T(8,128)(2,1)S(1)} %collective-permute-done.3.c_ref), channel_id=1, source_target_pairs={{0,1},{1,0},{2,3},{3,2},{4,5},{5,4},{6,7},{7,6},{8,9},{9,8},{10,11... | collective-permute-start | bytes 1671176 | tf_op jit(solution)/shard_map/ppermute | solution.py:370
  76.3 1.7 collective-permute-start.5
  78.0 96.2 %copy-start = (f32[2048]{0:T(1024)S(1)}, f32[2048]{0:T(1024)}, u32[]{:S(2)}) copy-start(f32[2048]{0:T(1024)} %param.16) | copy-start | bytes 24580
  146.0 1.3 collective-permute-start.6

commit v2 on v1

--- a/solution.py
+++ b/solution.py
@@ -13,6 +13,7 @@
 GRP_EP = ("grp", "zh", "zl", "core")
 LANES = 128
 CLASSES = 4
+CHUNKS = 4
 EPSILON = 1e-06
 F32 = jnp.float32
 BF16 = jnp.bfloat16
@@ -151,12 +152,19 @@
     topk, sizes, at_ref, a_ref, b_ref, c_ref, d_ref, wg_hbm, wu_hbm, wd_hbm,
     rank_ref, keep_ref, send_ref, load_ref, level_ref, wg_ref, wu_ref, wd_ref, sems,
 ):
-    copies = [
-        pltpu.make_async_copy(src.at[0], dst, sems.at[i])
-        for i, (src, dst) in enumerate(((wg_hbm, wg_ref), (wu_hbm, wu_ref), (wd_hbm, wd_ref)))
-    ]
-    copies[0].start()
-    copies[1].start()
+    copies = []
+    for i, (src, dst) in enumerate(((wg_hbm, wg_ref), (wu_hbm, wu_ref), (wd_hbm, wd_ref))):
+        step = dst.shape[0] // CHUNKS
+        copies.append(
+            [
+                pltpu.make_async_copy(
+                    src.at[0, pl.ds(c * step, step)], dst.at[pl.ds(c * step, step)], sems.at[i, c]
+                )
+                for c in range(CHUNKS)
+            ]
+        )
+    for copy in sum(copies, []):
+        copy.start()
     width = wg_ref.shape[0]
     is_core = at_ref[1] == 1
     is_odd = at_ref[2] == 1
@@ -224,13 +232,15 @@
             pick[:, k * part : (k + 1) * part], ref[:, :width], preferred_element_type=F32
         )
     picked = picked.astype(BF16)
-    copies[0].wait()
-    copies[2].start()
+    for copy in copies[0]:
+        copy.wait()
     gate_val = jnp.dot(picked, wg_ref[...], preferred_element_type=F32)
-    copies[1].wait()
+    for copy in copies[1]:
+        copy.wait()
     up_val = jnp.dot(picked, wu_ref[...], preferred_element_type=F32)
     act = (gate_val * jax.nn.sigmoid(gate_val) * up_val * gate).astype(BF16)
-    copies[2].wait()
+    for copy in copies[2]:
+        copy.wait()
     result = jnp.dot(act, wd_ref[...], preferred_element_type=F32)
     result = jnp.transpose(result).reshape(chips, 2, cols, slots)
     even, odd = result[:, 0], result[:, 1]
@@ -290,7 +300,7 @@
     def step(s, acc):
         return add(s, acc, keys(s))
 
-    out = lax.fori_loop(0, chips, step, jnp.zeros((cols, total), F32), unroll=8)
+    out = lax.fori_loop(0, chips, step, jnp.zeros((cols, total), F32), unroll=4)
     if pooled:
 
         def more(s, acc):
@@ -388,7 +398,7 @@
             pltpu.VMEM(w_gate.shape[1:], BF16),
             pltpu.VMEM(w_up.shape[1:], BF16),
             pltpu.VMEM(w_down.shape[1:], BF16),
-            pltpu.SemaphoreType.DMA((3,)),
+            pltpu.SemaphoreType.DMA((3, CHUNKS)),
         ],
         compiler_params=pltpu.CompilerParams(vmem_limit_bytes=50 << 20),
     )(at, *pieces, w_gate, w_up, w_down)

time: 177 us -> 170 us (0.960)
  blocking collectives: 148 us -> 143 us
    all_to_all x1, blocking collectives: 64.7 us -> 59 us  [run(): lax.all_to_all(both, CHIPS, split_axis=0, concat_axis=0, tiled=True)]
where the time goes in v2:
time: 170 us
  blocking collectives  143 us (84%)
  Pallas kernels  11.7 us (7%)
  waiting for transfers between devices  11.6 us (7%)
  starting transfers between devices  3.27 us (2%)
    all_to_all x1, blocking collectives, run(): lax.all_to_all(both, CHIPS, split_axis=0, concat_axis=0, tiled=True)  59 us
    all_gather x1, blocking collectives, shards(): own = lax.all_gather(payload, 'zh', axis=0, tiled=True)  56.7 us
    all_to_all x1, blocking collectives, shards(): lax.all_to_all(spread, CHIPS, split_axis=0, concat_axis=0, tiled=True)  26.8 us
    ppermute x1, waiting for transfers between devices, shards(): near = lax.ppermute(own, EP, zigzag)  7.88 us
    pallas_call x1, Pallas kernels, shards(): pl.pallas_call(functools.partial(experts_kernel, topk, sizes), in_specs=[...  4.89 us
  transfers between devices with their start and end apart: 5, of which 4 were waited for; matrix products, arithmetic and copies ran while one was open for 0% of the time, Pallas kernels for 0%

profile of v2, /device:TPU:46, one launch (start us, length us, event | category | flops | bytes accessed | tf_op | source)
XLA Modules:
  0.0 169.9 jit_solution(7791345624633752865)
XLA Ops:
  0.0 1.5 shard_map.82
  1.5 56.7 %all_gather.3.a_ref = bf16[128,2176]{1,0:T(8,128)(2,1)S(1)} all-gather(bf16[8,2176]{1,0:T(8,128)(2,1)} %shard_map.82), channel_id=1, replica_groups=mesh['grp'=4,'zh'=16,'zl'=2,'core'=2] {'zh'}, dimensions={0}, use_global_device_ids=true | all-gather | bytes 591872 | tf_op jit(solution)/shard_map/all_gather | solution.py:377
  58.2 2.9 %collective-permute-start.3 = (bf16[128,2176]{1,0:T(8,128)(2,1)S(1)}, bf16[128,2176]{1,0:T(8,128)(2,1)S(1)}, u32[]{:S(2)}, u32[]{:S(2)}) collective-permute-start(bf16[128,2176]{1,0:T(8,128)(2,1)S(1)} %all_gather.3.a_ref), channel_id=1, source_target_pairs={{0,2},{1,63},{2,4},{3,1},{4,6},{5,3},{6,8},{7,5},{8,10},{9,7},{10,... | collective-permute-start | bytes 1671176 | tf_op jit(solution)/shard_map/ppermute | solution.py:378
  61.1 0.0 collective-permute-start.2
  61.1 7.9 %collective-permute-done.3.c_ref = bf16[128,2176]{1,0:T(8,128)(2,1)S(1)} collective-permute-done((bf16[128,2176]{1,0:T(8,128)(2,1)S(1)}, bf16[128,2176]{1,0:T(8,128)(2,1)S(1)}, u32[]{:S(2)}, u32[]{:S(2)}) %collective-permute-start.3) | collective-permute-done | bytes 557088 | tf_op jit(solution)/shard_map/ppermute | solution.py:378
  68.9 0.0 collective-permute-start.4
  69.0 0.1 pad_add_fusion.at_ref
  69.0 0.0 collective-permute-done.2.b_ref
  69.0 1.9 %collective-permute-done.4.d_ref = bf16[128,2176]{1,0:T(8,128)(2,1)S(1)} collective-permute-done((bf16[128,2176]{1,0:T(8,128)(2,1)S(1)}, bf16[128,2176]{1,0:T(8,128)(2,1)S(1)}, u32[]{:S(2)}, u32[]{:S(2)}) %collective-permute-start.4) | collective-permute-done | bytes 557088 | tf_op jit(solution)/shard_map/ppermute | solution.py:380
  70.9 4.9 %shard_map.83 = (f32[64,512]{1,0:T(8,128)S(1)}, bf16[32,32,128]{2,1,0:T(8,128)(2,1)S(1)}, bf16[32,32,128]{2,1,0:T(8,128)(2,1)S(1)}, f32[64,128]{1,0:T(8,128)S(1)}, s32[1]{0:T(128)}) custom-call(s32[3]{0:T(128)S(1)} %pad_add_fusion.at_ref, bf16[128,2176]{1,0:T(8,128)(2,1)S(1)} %all_gather.3.a_ref, bf16[128,2176]{1,0:T(8,128)(2,1)S(1)} %collective-permute-done.2.b_ref, ...), custom_call_target="tpu_custom_call" | custom-call | tf_op jit(solution)/shard_map/pallas_call | solution.py:386
  75.8 0.3 collective-permute-start.5
  76.7 0.7 collective-permute-done.5
  77.5 0.0 copy-start
  77.5 62.9 %conditional.1 = ((f32[32,512]{1,0:T(8,128)S(1)}, f32[1,512]{1,0:T(1,128)S(1)})) conditional(s32[]{:T(128)} %bitcast.6, (s32[3]{0:T(128)S(1)}, bf16[32,32,128]{2,1,0:T(8,128)(2,1)S(1)}, bf16[32,32,128]{2,1,0:T(8,128)(2,1)S(1)}, f32[64,512]{1,0:T(8,128)S(1)}, f32[64,128]{1,0:T(8,128)S(1)}) %tuple.17, (s32[3]{0:T(128)S(1)}, ...), branch_computations={%region_0.0_spmd, %region_1.0_spmd, %region_2.0_spmd, %region_3.0_... | conditional | bytes 1704024 | solution.py:454
  77.5 0.8 branch_0_fun.2
  78.3 59.0 %all_to_all.21.rows_ref = bf16[32,40,128]{2,1,0:T(8,128)(2,1)S(1)} all-to-all(bf16[32,40,128]{2,1,0:T(8,128)(2,1)S(1)} %branch_0_fun.2), channel_id=1, replica_groups=mesh['grp'=4,'zh'=16,'zl'=2,'core'=2] {'zh','zl'}, dimensions={0} | all-to-all | bytes 655360 | tf_op jit(solution)/shard_map/cond/branch_0_fun/all_to_all | solution.py:440
  137.3 3.0 %branch_0_fun.3 = (f32[32,512]{1,0:T(8,128)S(1)}, f32[1,512]{1,0:T(1,128)S(1)}) custom-call(s32[3]{0:T(128)S(1)} %get-tuple-element.45.at_ref.took_ref, bf16[32,40,128]{2,1,0:T(8,128)(2,1)S(1)} %all_to_all.21.rows_ref, f32[64,512]{1,0:T(8,128)S(1)} %get-tuple-element.48.rank_ref, f32[64,128]{1,0:T(8,128)S(1)} %get-tuple-element.49.load_ref), custom_call_target="tpu_custom_call" | custom-call | tf_op jit(solution)/shard_map/cond/branch_0_fun/pallas_call | solution.py:441
  140.4 0.1 collective-permute-start.6
  140.5 1.1 collective-permute-done.6.other_ref
  141.7 26.8 %all_to_all.25.squares_ref = bf16[32,4,128]{2,1,0:T(4,128)(2,1)S(1)} all-to-all(bf16[32,4,128]{2,1,0:T(4,128)(2,1)S(1)} %shard_map.84), channel_id=1, replica_groups=mesh['grp'=4,'zh'=16,'zl'=2,'core'=2] {'zh','zl'}, dimensions={0} | all-to-all | bytes 65536 | tf_op jit(solution)/shard_map/all_to_all | solution.py:466
  168.5 0.0 copy-done
  168.5 1.4 shard_map.85
  (1 shorter events, 0.0 us)
Async XLA Ops:
  58.2 10.7 %collective-permute-start.3 = (bf16[128,2176]{1,0:T(8,128)(2,1)S(1)}, bf16[128,2176]{1,0:T(8,128)(2,1)S(1)}, u32[]{:S(2)}, u32[]{:S(2)}) collective-permute-start(bf16[128,2176]{1,0:T(8,128)(2,1)S(1)} %all_gather.3.a_ref), channel_id=1, source_target_pairs={{0,2},{1,63},{2,4},{3,1},{4,6},{5,3},{6,8},{7,5},{8,10},{9,7},{10,... | collective-permute-start | bytes 1671176 | tf_op jit(solution)/shard_map/ppermute | solution.py:378
  61.1 8.0 %collective-permute-start.2 = (bf16[128,2176]{1,0:T(8,128)(2,1)S(1)}, bf16[128,2176]{1,0:T(8,128)(2,1)S(1)}, u32[]{:S(2)}, u32[]{:S(2)}) collective-permute-start(bf16[128,2176]{1,0:T(8,128)(2,1)S(1)} %all_gather.3.a_ref), channel_id=1, source_target_pairs={{0,1},{1,0},{2,3},{3,2},{4,5},{5,4},{6,7},{7,6},{8,9},{9,8},{10,11... | collective-permute-start | bytes 1671176 | tf_op jit(solution)/shard_map/ppermute | solution.py:379
  68.9 2.0 %collective-permute-start.4 = (bf16[128,2176]{1,0:T(8,128)(2,1)S(1)}, bf16[128,2176]{1,0:T(8,128)(2,1)S(1)}, u32[]{:S(2)}, u32[]{:S(2)}) collective-permute-start(bf16[128,2176]{1,0:T(8,128)(2,1)S(1)} %collective-permute-done.3.c_ref), channel_id=1, source_target_pairs={{0,1},{1,0},{2,3},{3,2},{4,5},{5,4},{6,7},{7,6},{8,9},{9,8},{10,11... | collective-permute-start | bytes 1671176 | tf_op jit(solution)/shard_map/ppermute | solution.py:380
  75.8 1.7 collective-permute-start.5
  77.5 91.1 %copy-start = (f32[2048]{0:T(1024)S(1)}, f32[2048]{0:T(1024)}, u32[]{:S(2)}) copy-start(f32[2048]{0:T(1024)} %param.16) | copy-start | bytes 24580
  140.4 1.3 collective-permute-start.6

commit v3 on v2

--- a/solution.py
+++ b/solution.py
@@ -267,8 +267,7 @@
     extra = capacity - LANES
     groups = LANES // extra
     each = cols // groups
-    row = lax.broadcasted_iota(jnp.int32, (2 * LANES, total), 0)
-    slot = jnp.where(row < LANES, row, LANES + (row - LANES) % extra).astype(F32).astype(BF16)
+    slot = lax.broadcasted_iota(jnp.int32, (capacity, total), 0).astype(F32).astype(BF16)
     col = lax.broadcasted_iota(jnp.int32, (cols, LANES), 0)
     lane = lax.broadcasted_iota(jnp.int32, (cols, LANES), 1)
     own = (col // each) == (lane // extra)
@@ -282,6 +281,7 @@
 
     def add(s, acc, hit):
         pick = jnp.where(hit, one, zero)
+        pick = jnp.concatenate([pick[:LANES]] + [pick[LANES:]] * groups, axis=0)
         block = rows_ref[s].astype(F32)
         tail = jnp.concatenate([block[cols:]] * groups, axis=0)
         tail = jnp.where(own, tail, 0.0)
@@ -300,7 +300,7 @@
     def step(s, acc):
         return add(s, acc, keys(s))
 
-    out = lax.fori_loop(0, chips, step, jnp.zeros((cols, total), F32), unroll=4)
+    out = lax.fori_loop(0, chips, step, jnp.zeros((cols, total), F32), unroll=8)
     if pooled:
 
         def more(s, acc):

time: 170 us -> 177 us (1.041)
  the two profiles are of different devices: /device:TPU:46 before, /device:TPU:38 now
where the time goes in v3:
time: 177 us; the launch traced here: 178 us
  blocking collectives  142 us (80%)
  waiting for transfers between devices  15.3 us (9%)
  Pallas kernels  13.5 us (8%)
  starting transfers between devices  6.62 us (4%)
    all_to_all x1, blocking collectives, run(): lax.all_to_all(both, CHIPS, split_axis=0, concat_axis=0, tiled=True)  58.3 us
    all_gather x1, blocking collectives, shards(): own = lax.all_gather(payload, 'zh', axis=0, tiled=True)  56.7 us
    all_to_all x1, blocking collectives, shards(): lax.all_to_all(spread, CHIPS, split_axis=0, concat_axis=0, tiled=True)  26.8 us
    ppermute x1, waiting for transfers between devices, shards(): near = lax.ppermute(own, EP, zigzag)  7.88 us
    pallas_call x1, Pallas kernels, shards(): pl.pallas_call(functools.partial(experts_kernel, topk, sizes), in_specs=[...  4.89 us
  transfers between devices with their start and end apart: 7, of which 6 were waited for; matrix products, arithmetic and copies ran while one was open for 0% of the time, Pallas kernels for 0%

profile of v3, /device:TPU:38, one launch (start us, length us, event | category | flops | bytes accessed | tf_op | source)
XLA Modules:
  0.0 178.0 jit_solution(3801480846292885571)
XLA Ops:
  0.0 1.5 shard_map.82
  1.5 56.7 %all_gather.3.a_ref = bf16[128,2176]{1,0:T(8,128)(2,1)S(1)} all-gather(bf16[8,2176]{1,0:T(8,128)(2,1)} %shard_map.82), channel_id=1, replica_groups=mesh['grp'=4,'zh'=16,'zl'=2,'core'=2] {'zh'}, dimensions={0}, use_global_device_ids=true | all-gather | bytes 591872 | tf_op jit(solution)/shard_map/all_gather | solution.py:377
  58.2 2.9 %collective-permute-start.3 = (bf16[128,2176]{1,0:T(8,128)(2,1)S(1)}, bf16[128,2176]{1,0:T(8,128)(2,1)S(1)}, u32[]{:S(2)}, u32[]{:S(2)}) collective-permute-start(bf16[128,2176]{1,0:T(8,128)(2,1)S(1)} %all_gather.3.a_ref), channel_id=1, source_target_pairs={{0,2},{1,63},{2,4},{3,1},{4,6},{5,3},{6,8},{7,5},{8,10},{9,7},{10,... | collective-permute-start | bytes 1671176 | tf_op jit(solution)/shard_map/ppermute | solution.py:378
  61.1 0.0 collective-permute-start.2
  61.1 7.9 %collective-permute-done.3.c_ref = bf16[128,2176]{1,0:T(8,128)(2,1)S(1)} collective-permute-done((bf16[128,2176]{1,0:T(8,128)(2,1)S(1)}, bf16[128,2176]{1,0:T(8,128)(2,1)S(1)}, u32[]{:S(2)}, u32[]{:S(2)}) %collective-permute-start.3) | collective-permute-done | bytes 557088 | tf_op jit(solution)/shard_map/ppermute | solution.py:378
  68.9 0.0 collective-permute-start.4
  69.0 0.1 pad_add_fusion.at_ref
  69.0 0.0 collective-permute-done.2.b_ref
  69.0 1.9 %collective-permute-done.4.d_ref = bf16[128,2176]{1,0:T(8,128)(2,1)S(1)} collective-permute-done((bf16[128,2176]{1,0:T(8,128)(2,1)S(1)}, bf16[128,2176]{1,0:T(8,128)(2,1)S(1)}, u32[]{:S(2)}, u32[]{:S(2)}) %collective-permute-start.4) | collective-permute-done | bytes 557088 | tf_op jit(solution)/shard_map/ppermute | solution.py:380
  70.9 4.9 %shard_map.83 = (f32[64,512]{1,0:T(8,128)S(1)}, bf16[32,32,128]{2,1,0:T(8,128)(2,1)S(1)}, bf16[32,32,128]{2,1,0:T(8,128)(2,1)S(1)}, f32[64,128]{1,0:T(8,128)S(1)}, s32[1]{0:T(128)}) custom-call(s32[3]{0:T(128)S(1)} %pad_add_fusion.at_ref, bf16[128,2176]{1,0:T(8,128)(2,1)S(1)} %all_gather.3.a_ref, bf16[128,2176]{1,0:T(8,128)(2,1)S(1)} %collective-permute-done.2.b_ref, ...), custom_call_target="tpu_custom_call" | custom-call | tf_op jit(solution)/shard_map/pallas_call | solution.py:386
  75.8 0.3 collective-permute-start.5
  76.7 0.7 collective-permute-done.5
  77.5 0.0 copy-start
  77.5 71.0 %conditional.1 = ((f32[32,512]{1,0:T(8,128)S(1)}, f32[1,512]{1,0:T(1,128)S(1)})) conditional(s32[]{:T(128)} %bitcast.6, (s32[3]{0:T(128)S(1)}, bf16[32,32,128]{2,1,0:T(8,128)(2,1)S(1)}, bf16[32,32,128]{2,1,0:T(8,128)(2,1)S(1)}, f32[64,512]{1,0:T(8,128)S(1)}, f32[64,128]{1,0:T(8,128)S(1)}) %tuple.17, (s32[3]{0:T(128)S(1)}, ...), branch_computations={%region_0.0_spmd, %region_1.0_spmd, %region_2.0_spmd, %region_3.0_... | conditional | bytes 1704024 | solution.py:454
  77.5 0.7 branch_2_fun.3
  78.2 1.8 collective-permute-start
  80.0 1.6 collective-permute-start.1
  81.6 3.5 %collective-permute-done.right_ref = bf16[512,128]{1,0:T(8,128)(2,1)S(1)} collective-permute-done((bf16[512,128]{1,0:T(8,128)(2,1)S(1)}, bf16[512,128]{1,0:T(8,128)(2,1)S(1)}, u32[]{:S(2)}, u32[]{:S(2)}) %collective-permute-start) | collective-permute-done | bytes 131104 | tf_op jit(solution)/shard_map/cond/branch_2_fun/ppermute | solution.py:431
  85.1 0.2 collective-permute-done.1.left_ref
  85.2 1.4 branch_2_fun.4
  86.6 58.3 %all_to_all.23.rows_ref = bf16[32,40,128]{2,1,0:T(8,128)(2,1)S(1)} all-to-all(bf16[32,40,128]{2,1,0:T(8,128)(2,1)S(1)} %get-tuple-element.62), channel_id=1, replica_groups=mesh['grp'=4,'zh'=16,'zl'=2,'core'=2] {'zh','zl'}, dimensions={0} | all-to-all | bytes 655360 | tf_op jit(solution)/shard_map/cond/branch_2_fun/all_to_all | solution.py:440
  145.0 3.5 %branch_2_fun.5 = (f32[32,512]{1,0:T(8,128)S(1)}, f32[1,512]{1,0:T(1,128)S(1)}) custom-call(s32[2]{0:T(128)S(1)} %get-tuple-element.61.took_ref, bf16[32,40,128]{2,1,0:T(8,128)(2,1)S(1)} %all_to_all.23.rows_ref, f32[64,512]{1,0:T(8,128)S(1)} %get-tuple-element.63.rank_ref, f32[64,128]{1,0:T(8,128)S(1)} %get-tuple-element.60.load_ref), custom_call_target="tpu_custom_call" | custom-call | tf_op jit(solution)/shard_map/cond/branch_2_fun/pallas_call | solution.py:441
  148.5 0.1 collective-permute-start.6
  148.7 1.1 collective-permute-done.6.other_ref
  149.8 26.8 %all_to_all.25.squares_ref = bf16[32,4,128]{2,1,0:T(4,128)(2,1)S(1)} all-to-all(bf16[32,4,128]{2,1,0:T(4,128)(2,1)S(1)} %shard_map.84), channel_id=1, replica_groups=mesh['grp'=4,'zh'=16,'zl'=2,'core'=2] {'zh','zl'}, dimensions={0} | all-to-all | bytes 65536 | tf_op jit(solution)/shard_map/all_to_all | solution.py:466
  176.6 0.0 copy-done
  176.6 1.4 shard_map.85
  (1 shorter events, 0.0 us)
Async XLA Ops:
  58.2 10.7 %collective-permute-start.3 = (bf16[128,2176]{1,0:T(8,128)(2,1)S(1)}, bf16[128,2176]{1,0:T(8,128)(2,1)S(1)}, u32[]{:S(2)}, u32[]{:S(2)}) collective-permute-start(bf16[128,2176]{1,0:T(8,128)(2,1)S(1)} %all_gather.3.a_ref), channel_id=1, source_target_pairs={{0,2},{1,63},{2,4},{3,1},{4,6},{5,3},{6,8},{7,5},{8,10},{9,7},{10,... | collective-permute-start | bytes 1671176 | tf_op jit(solution)/shard_map/ppermute | solution.py:378
  61.1 8.0 %collective-permute-start.2 = (bf16[128,2176]{1,0:T(8,128)(2,1)S(1)}, bf16[128,2176]{1,0:T(8,128)(2,1)S(1)}, u32[]{:S(2)}, u32[]{:S(2)}) collective-permute-start(bf16[128,2176]{1,0:T(8,128)(2,1)S(1)} %all_gather.3.a_ref), channel_id=1, source_target_pairs={{0,1},{1,0},{2,3},{3,2},{4,5},{5,4},{6,7},{7,6},{8,9},{9,8},{10,11... | collective-permute-start | bytes 1671176 | tf_op jit(solution)/shard_map/ppermute | solution.py:379
  68.9 2.0 %collective-permute-start.4 = (bf16[128,2176]{1,0:T(8,128)(2,1)S(1)}, bf16[128,2176]{1,0:T(8,128)(2,1)S(1)}, u32[]{:S(2)}, u32[]{:S(2)}) collective-permute-start(bf16[128,2176]{1,0:T(8,128)(2,1)S(1)} %collective-permute-done.3.c_ref), channel_id=1, source_target_pairs={{0,1},{1,0},{2,3},{3,2},{4,5},{5,4},{6,7},{7,6},{8,9},{9,8},{10,11... | collective-permute-start | bytes 1671176 | tf_op jit(solution)/shard_map/ppermute | solution.py:380
  75.8 1.7 collective-permute-start.5
  77.5 99.2 %copy-start = (f32[2048]{0:T(1024)S(1)}, f32[2048]{0:T(1024)}, u32[]{:S(2)}) copy-start(f32[2048]{0:T(1024)} %param.16) | copy-start | bytes 24580
  78.2 6.9 %collective-permute-start = (bf16[512,128]{1,0:T(8,128)(2,1)S(1)}, bf16[512,128]{1,0:T(8,128)(2,1)S(1)}, u32[]{:S(2)}, u32[]{:S(2)}) collective-permute-start(bf16[512,128]{1,0:T(8,128)(2,1)S(1)} %get-tuple-element.58), channel_id=1, source_target_pairs={{0,2},{1,3},{2,4},{3,5},{4,6},{5,7},{6,8},{7,9},{8,10},{9,11},{10,... | collective-permute-start | bytes 393224 | tf_op jit(solution)/shard_map/cond/branch_2_fun/ppermute | solution.py:431
  80.0 5.3 %collective-permute-start.1 = (bf16[512,128]{1,0:T(8,128)(2,1)S(1)}, bf16[512,128]{1,0:T(8,128)(2,1)S(1)}, u32[]{:S(2)}, u32[]{:S(2)}) collective-permute-start(bf16[512,128]{1,0:T(8,128)(2,1)S(1)} %get-tuple-element.59), channel_id=1, source_target_pairs={{0,62},{1,63},{2,0},{3,1},{4,2},{5,3},{6,4},{7,5},{8,6},{9,7},{10,... | collective-permute-start | bytes 393224 | tf_op jit(solution)/shard_map/cond/branch_2_fun/ppermute | solution.py:431
  148.5 1.3 collective-permute-start.6

commit v4 on v3

--- a/solution.py
+++ b/solution.py
@@ -14,6 +14,7 @@
 LANES = 128
 CLASSES = 4
 CHUNKS = 4
+BATCH = 8
 EPSILON = 1e-06
 F32 = jnp.float32
 BF16 = jnp.bfloat16
@@ -297,10 +298,27 @@
         high = jnp.where(high < 0.0, -1.0, capacity - 1.0 - high)
         return (slot == low.astype(BF16)) | (slot == high.astype(BF16))
 
-    def step(s, acc):
-        return add(s, acc, keys(s))
-
-    out = lax.fori_loop(0, chips, step, jnp.zeros((cols, total), F32), unroll=8)
+    def step(i, acc):
+        mains, tails, main_picks, tail_picks = [], [], [], []
+        for first in range(0, BATCH, groups):
+            spread = jnp.zeros((cols, LANES), F32)
+            for q in range(groups):
+                s = i * BATCH + first + q
+                pick = jnp.where(keys(s), one, zero)
+                main_picks.append(pick[:LANES])
+                tail_picks.append(pick[LANES:])
+                block = rows_ref[s].astype(F32)
+                mains.append(block[:cols])
+                tail = block[cols:]
+                turned = [tail] + [pltpu.roll(tail, k * extra, 1) for k in range(1, groups)]
+                tail = jnp.concatenate([turned[(q - g) % groups] for g in range(groups)], axis=0)
+                spread = jnp.where(lane // extra == q, tail, spread)
+            tails.append(spread)
+        left = jnp.concatenate(mains + tails, axis=1).astype(BF16)
+        pick = jnp.concatenate(main_picks + tail_picks, axis=0)
+        return acc + jnp.dot(left, pick, preferred_element_type=F32)
+
+    out = lax.fori_loop(0, chips // BATCH, step, jnp.zeros((cols, total), F32), unroll=2)
     if pooled:
 
         def more(s, acc):

time: 177 us -> 176 us (level)
  the two profiles are of different devices: /device:TPU:38 before, /device:TPU:46 now
where the time goes in v4:
time: 176 us; the launch traced here: 177 us
  blocking collectives  142 us (81%)
  waiting for transfers between devices  15.3 us (9%)
  Pallas kernels  12.7 us (7%)
  starting transfers between devices  6.62 us (4%)
    all_to_all x1, blocking collectives, run(): lax.all_to_all(both, CHIPS, split_axis=0, concat_axis=0, tiled=True)  58.3 us
    all_gather x1, blocking collectives, shards(): own = lax.all_gather(payload, 'zh', axis=0, tiled=True)  56.7 us
    all_to_all x1, blocking collectives, shards(): lax.all_to_all(spread, CHIPS, split_axis=0, concat_axis=0, tiled=True)  26.8 us
    ppermute x1, waiting for transfers between devices, shards(): near = lax.ppermute(own, EP, zigzag)  7.88 us
    pallas_call x1, Pallas kernels, shards(): pl.pallas_call(functools.partial(experts_kernel, topk, sizes), in_specs=[...  4.89 us
  transfers between devices with their start and end apart: 7, of which 6 were waited for; matrix products, arithmetic and copies ran while one was open for 0% of the time, Pallas kernels for 0%

profile of v4, /device:TPU:46, one launch (start us, length us, event | category | flops | bytes accessed | tf_op | source)
XLA Modules:
  0.0 177.3 jit_solution(16469563469538555755)
XLA Ops:
  0.0 1.5 shard_map.82
  1.5 56.7 %all_gather.3.a_ref = bf16[128,2176]{1,0:T(8,128)(2,1)S(1)} all-gather(bf16[8,2176]{1,0:T(8,128)(2,1)} %shard_map.82), channel_id=1, replica_groups=mesh['grp'=4,'zh'=16,'zl'=2,'core'=2] {'zh'}, dimensions={0}, use_global_device_ids=true | all-gather | bytes 591872 | tf_op jit(solution)/shard_map/all_gather | solution.py:395
  58.2 2.9 %collective-permute-start.3 = (bf16[128,2176]{1,0:T(8,128)(2,1)S(1)}, bf16[128,2176]{1,0:T(8,128)(2,1)S(1)}, u32[]{:S(2)}, u32[]{:S(2)}) collective-permute-start(bf16[128,2176]{1,0:T(8,128)(2,1)S(1)} %all_gather.3.a_ref), channel_id=1, source_target_pairs={{0,2},{1,63},{2,4},{3,1},{4,6},{5,3},{6,8},{7,5},{8,10},{9,7},{10,... | collective-permute-start | bytes 1671176 | tf_op jit(solution)/shard_map/ppermute | solution.py:396
  61.1 0.0 collective-permute-start.2
  61.1 7.9 %collective-permute-done.3.c_ref = bf16[128,2176]{1,0:T(8,128)(2,1)S(1)} collective-permute-done((bf16[128,2176]{1,0:T(8,128)(2,1)S(1)}, bf16[128,2176]{1,0:T(8,128)(2,1)S(1)}, u32[]{:S(2)}, u32[]{:S(2)}) %collective-permute-start.3) | collective-permute-done | bytes 557088 | tf_op jit(solution)/shard_map/ppermute | solution.py:396
  68.9 0.0 collective-permute-start.4
  69.0 0.1 pad_add_fusion.at_ref
  69.0 0.0 collective-permute-done.2.b_ref
  69.0 1.9 %collective-permute-done.4.d_ref = bf16[128,2176]{1,0:T(8,128)(2,1)S(1)} collective-permute-done((bf16[128,2176]{1,0:T(8,128)(2,1)S(1)}, bf16[128,2176]{1,0:T(8,128)(2,1)S(1)}, u32[]{:S(2)}, u32[]{:S(2)}) %collective-permute-start.4) | collective-permute-done | bytes 557088 | tf_op jit(solution)/shard_map/ppermute | solution.py:398
  70.9 4.9 %shard_map.83 = (f32[64,512]{1,0:T(8,128)S(1)}, bf16[32,32,128]{2,1,0:T(8,128)(2,1)S(1)}, bf16[32,32,128]{2,1,0:T(8,128)(2,1)S(1)}, f32[64,128]{1,0:T(8,128)S(1)}, s32[1]{0:T(128)}) custom-call(s32[3]{0:T(128)S(1)} %pad_add_fusion.at_ref, bf16[128,2176]{1,0:T(8,128)(2,1)S(1)} %all_gather.3.a_ref, bf16[128,2176]{1,0:T(8,128)(2,1)S(1)} %collective-permute-done.2.b_ref, ...), custom_call_target="tpu_custom_call" | custom-call | tf_op jit(solution)/shard_map/pallas_call | solution.py:404
  75.8 0.3 collective-permute-start.5
  76.7 0.7 collective-permute-done.5
  77.5 0.0 copy-start
  77.5 70.3 %conditional.1 = ((f32[32,512]{1,0:T(8,128)S(1)}, f32[1,512]{1,0:T(1,128)S(1)})) conditional(s32[]{:T(128)} %bitcast.6, (s32[3]{0:T(128)S(1)}, bf16[32,32,128]{2,1,0:T(8,128)(2,1)S(1)}, bf16[32,32,128]{2,1,0:T(8,128)(2,1)S(1)}, f32[64,512]{1,0:T(8,128)S(1)}, f32[64,128]{1,0:T(8,128)S(1)}) %tuple.17, (s32[3]{0:T(128)S(1)}, ...), branch_computations={%region_0.0_spmd, %region_1.0_spmd, %region_2.0_spmd, %region_3.0_... | conditional | bytes 1704024 | solution.py:472
  77.5 0.7 branch_2_fun.3
  78.2 1.8 collective-permute-start
  80.0 1.6 collective-permute-start.1
  81.6 3.5 %collective-permute-done.right_ref = bf16[512,128]{1,0:T(8,128)(2,1)S(1)} collective-permute-done((bf16[512,128]{1,0:T(8,128)(2,1)S(1)}, bf16[512,128]{1,0:T(8,128)(2,1)S(1)}, u32[]{:S(2)}, u32[]{:S(2)}) %collective-permute-start) | collective-permute-done | bytes 131104 | tf_op jit(solution)/shard_map/cond/branch_2_fun/ppermute | solution.py:449
  85.1 0.2 collective-permute-done.1.left_ref
  85.2 1.4 branch_2_fun.4
  86.6 58.3 %all_to_all.23.rows_ref = bf16[32,40,128]{2,1,0:T(8,128)(2,1)S(1)} all-to-all(bf16[32,40,128]{2,1,0:T(8,128)(2,1)S(1)} %get-tuple-element.62), channel_id=1, replica_groups=mesh['grp'=4,'zh'=16,'zl'=2,'core'=2] {'zh','zl'}, dimensions={0} | all-to-all | bytes 655360 | tf_op jit(solution)/shard_map/cond/branch_2_fun/all_to_all | solution.py:458
  145.0 2.8 %branch_2_fun.5 = (f32[32,512]{1,0:T(8,128)S(1)}, f32[1,512]{1,0:T(1,128)S(1)}) custom-call(s32[2]{0:T(128)S(1)} %get-tuple-element.61.took_ref, bf16[32,40,128]{2,1,0:T(8,128)(2,1)S(1)} %all_to_all.23.rows_ref, f32[64,512]{1,0:T(8,128)S(1)} %get-tuple-element.63.rank_ref, f32[64,128]{1,0:T(8,128)S(1)} %get-tuple-element.60.load_ref), custom_call_target="tpu_custom_call" | custom-call | tf_op jit(solution)/shard_map/cond/branch_2_fun/pallas_call | solution.py:459
  147.8 0.1 collective-permute-start.6
  147.9 1.1 collective-permute-done.6.other_ref
  149.1 26.8 %all_to_all.25.squares_ref = bf16[32,4,128]{2,1,0:T(4,128)(2,1)S(1)} all-to-all(bf16[32,4,128]{2,1,0:T(4,128)(2,1)S(1)} %shard_map.84), channel_id=1, replica_groups=mesh['grp'=4,'zh'=16,'zl'=2,'core'=2] {'zh','zl'}, dimensions={0} | all-to-all | bytes 65536 | tf_op jit(solution)/shard_map/all_to_all | solution.py:484
  175.9 0.0 copy-done
  175.9 1.4 shard_map.85
  (1 shorter events, 0.0 us)
Async XLA Ops:
  58.2 10.7 %collective-permute-start.3 = (bf16[128,2176]{1,0:T(8,128)(2,1)S(1)}, bf16[128,2176]{1,0:T(8,128)(2,1)S(1)}, u32[]{:S(2)}, u32[]{:S(2)}) collective-permute-start(bf16[128,2176]{1,0:T(8,128)(2,1)S(1)} %all_gather.3.a_ref), channel_id=1, source_target_pairs={{0,2},{1,63},{2,4},{3,1},{4,6},{5,3},{6,8},{7,5},{8,10},{9,7},{10,... | collective-permute-start | bytes 1671176 | tf_op jit(solution)/shard_map/ppermute | solution.py:396
  61.1 8.0 %collective-permute-start.2 = (bf16[128,2176]{1,0:T(8,128)(2,1)S(1)}, bf16[128,2176]{1,0:T(8,128)(2,1)S(1)}, u32[]{:S(2)}, u32[]{:S(2)}) collective-permute-start(bf16[128,2176]{1,0:T(8,128)(2,1)S(1)} %all_gather.3.a_ref), channel_id=1, source_target_pairs={{0,1},{1,0},{2,3},{3,2},{4,5},{5,4},{6,7},{7,6},{8,9},{9,8},{10,11... | collective-permute-start | bytes 1671176 | tf_op jit(solution)/shard_map/ppermute | solution.py:397
  68.9 2.0 %collective-permute-start.4 = (bf16[128,2176]{1,0:T(8,128)(2,1)S(1)}, bf16[128,2176]{1,0:T(8,128)(2,1)S(1)}, u32[]{:S(2)}, u32[]{:S(2)}) collective-permute-start(bf16[128,2176]{1,0:T(8,128)(2,1)S(1)} %collective-permute-done.3.c_ref), channel_id=1, source_target_pairs={{0,1},{1,0},{2,3},{3,2},{4,5},{5,4},{6,7},{7,6},{8,9},{9,8},{10,11... | collective-permute-start | bytes 1671176 | tf_op jit(solution)/shard_map/ppermute | solution.py:398
  75.8 1.7 collective-permute-start.5
  77.5 98.4 %copy-start = (f32[2048]{0:T(1024)S(1)}, f32[2048]{0:T(1024)}, u32[]{:S(2)}) copy-start(f32[2048]{0:T(1024)} %param.16) | copy-start | bytes 24580
  78.2 6.9 %collective-permute-start = (bf16[512,128]{1,0:T(8,128)(2,1)S(1)}, bf16[512,128]{1,0:T(8,128)(2,1)S(1)}, u32[]{:S(2)}, u32[]{:S(2)}) collective-permute-start(bf16[512,128]{1,0:T(8,128)(2,1)S(1)} %get-tuple-element.58), channel_id=1, source_target_pairs={{0,2},{1,3},{2,4},{3,5},{4,6},{5,7},{6,8},{7,9},{8,10},{9,11},{10,... | collective-permute-start | bytes 393224 | tf_op jit(solution)/shard_map/cond/branch_2_fun/ppermute | solution.py:449
  80.0 5.3 %collective-permute-start.1 = (bf16[512,128]{1,0:T(8,128)(2,1)S(1)}, bf16[512,128]{1,0:T(8,128)(2,1)S(1)}, u32[]{:S(2)}, u32[]{:S(2)}) collective-permute-start(bf16[512,128]{1,0:T(8,128)(2,1)S(1)} %get-tuple-element.59), channel_id=1, source_target_pairs={{0,62},{1,63},{2,0},{3,1},{4,2},{5,3},{6,4},{7,5},{8,6},{9,7},{10,... | collective-permute-start | bytes 393224 | tf_op jit(solution)/shard_map/cond/branch_2_fun/ppermute | solution.py:449
  147.8 1.3 collective-permute-start.6

commit v5 on v4

--- a/solution.py
+++ b/solution.py
@@ -189,7 +189,7 @@
     for k in range(topk):
         match = match + jnp.where(ordered[k : k + 1, :] == expert, 1.0, 0.0)
     index = lax.broadcasted_iota(jnp.int32, (total, total), 0)
-    at = lax.broadcasted_iota(jnp.int32, (total, total), 1)
+    at = lax.broadcasted_iota(jnp.int32, (1, total), 1)
     place = at % part // per_dev * (per_dev * CLASSES) + at // part * per_dev + at % per_dev
     counts = match.astype(BF16)
     rank = jnp.dot(

time: 176 us -> 174 us (0.989)
  the two profiles are of different devices: /device:TPU:46 before, /device:TPU:37 now
where the time goes in v5:
time: 174 us
  blocking collectives  138 us (79%)
  starting transfers between devices  21.9 us (13%)
  Pallas kernels  10.5 us (6%)
  waiting for transfers between devices  2.84 us (2%)
    all_to_all x1, blocking collectives, run(): lax.all_to_all(both, CHIPS, split_axis=0, concat_axis=0, tiled=True)  62.8 us
    all_gather x1, blocking collectives, shards(): own = lax.all_gather(payload, 'zh', axis=0, tiled=True)  50.1 us
    all_to_all x1, blocking collectives, shards(): lax.all_to_all(spread, CHIPS, split_axis=0, concat_axis=0, tiled=True)  25.2 us
    ppermute x1, starting transfers between devices, shards(): own_pair = lax.ppermute(own, 'core', swap)  8.9 us
    ppermute x1, starting transfers between devices, shards(): near_pair = lax.ppermute(near, 'core', swap)  7.88 us
    pallas_call x1, Pallas kernels, shards(): pl.pallas_call(functools.partial(experts_kernel, topk, sizes), in_specs=[...  4.89 us
  transfers between devices with their start and end apart: 5, of which 3 were waited for; matrix products, arithmetic and copies ran while one was open for 0% of the time, Pallas kernels for 0%

profile of v5, /device:TPU:37, one launch (start us, length us, event | category | flops | bytes accessed | tf_op | source)
XLA Modules:
  0.0 174.1 jit_solution(16469563469538555755)
XLA Ops:
  0.0 1.5 shard_map.82
  1.5 50.1 %all_gather.3.a_ref = bf16[128,2176]{1,0:T(8,128)(2,1)S(1)} all-gather(bf16[8,2176]{1,0:T(8,128)(2,1)} %shard_map.82), channel_id=1, replica_groups=mesh['grp'=4,'zh'=16,'zl'=2,'core'=2] {'zh'}, dimensions={0}, use_global_device_ids=true | all-gather | bytes 591872 | tf_op jit(solution)/shard_map/all_gather | solution.py:395
  51.6 2.0 %collective-permute-start.3 = (bf16[128,2176]{1,0:T(8,128)(2,1)S(1)}, bf16[128,2176]{1,0:T(8,128)(2,1)S(1)}, u32[]{:S(2)}, u32[]{:S(2)}) collective-permute-start(bf16[128,2176]{1,0:T(8,128)(2,1)S(1)} %all_gather.3.a_ref), channel_id=1, source_target_pairs={{0,2},{1,63},{2,4},{3,1},{4,6},{5,3},{6,8},{7,5},{8,10},{9,7},{10,... | collective-permute-start | bytes 1671176 | tf_op jit(solution)/shard_map/ppermute | solution.py:396
  53.6 8.9 %collective-permute-start.2 = (bf16[128,2176]{1,0:T(8,128)(2,1)S(1)}, bf16[128,2176]{1,0:T(8,128)(2,1)S(1)}, u32[]{:S(2)}, u32[]{:S(2)}) collective-permute-start(bf16[128,2176]{1,0:T(8,128)(2,1)S(1)} %all_gather.3.a_ref), channel_id=1, source_target_pairs={{0,1},{1,0},{2,3},{3,2},{4,5},{5,4},{6,7},{7,6},{8,9},{9,8},{10,11... | collective-permute-start | bytes 1671176 | tf_op jit(solution)/shard_map/ppermute | solution.py:397
  62.5 0.0 collective-permute-done.3.c_ref
  62.5 7.9 %collective-permute-start.4 = (bf16[128,2176]{1,0:T(8,128)(2,1)S(1)}, bf16[128,2176]{1,0:T(8,128)(2,1)S(1)}, u32[]{:S(2)}, u32[]{:S(2)}) collective-permute-start(bf16[128,2176]{1,0:T(8,128)(2,1)S(1)} %collective-permute-done.3.c_ref), channel_id=1, source_target_pairs={{0,1},{1,0},{2,3},{3,2},{4,5},{5,4},{6,7},{7,6},{8,9},{9,8},{10,11... | collective-permute-start | bytes 1671176 | tf_op jit(solution)/shard_map/ppermute | solution.py:398
  70.4 0.1 pad_add_fusion.at_ref
  70.5 0.0 collective-permute-done.2.b_ref
  70.5 1.5 collective-permute-done.4.d_ref
  72.0 4.9 %shard_map.83 = (f32[64,512]{1,0:T(8,128)S(1)}, bf16[32,32,128]{2,1,0:T(8,128)(2,1)S(1)}, bf16[32,32,128]{2,1,0:T(8,128)(2,1)S(1)}, f32[64,128]{1,0:T(8,128)S(1)}, s32[1]{0:T(128)}) custom-call(s32[3]{0:T(128)S(1)} %pad_add_fusion.at_ref, bf16[128,2176]{1,0:T(8,128)(2,1)S(1)} %all_gather.3.a_ref, bf16[128,2176]{1,0:T(8,128)(2,1)S(1)} %collective-permute-done.2.b_ref, ...), custom_call_target="tpu_custom_call" | custom-call | tf_op jit(solution)/shard_map/pallas_call | solution.py:404
  76.9 0.5 collective-permute-start.5
  78.0 0.5 collective-permute-done.5
  78.5 0.0 copy-start
  78.5 65.5 %conditional.1 = ((f32[32,512]{1,0:T(8,128)S(1)}, f32[1,512]{1,0:T(1,128)S(1)})) conditional(s32[]{:T(128)} %bitcast.6, (s32[3]{0:T(128)S(1)}, bf16[32,32,128]{2,1,0:T(8,128)(2,1)S(1)}, bf16[32,32,128]{2,1,0:T(8,128)(2,1)S(1)}, f32[64,512]{1,0:T(8,128)S(1)}, f32[64,128]{1,0:T(8,128)S(1)}) %tuple.17, (s32[3]{0:T(128)S(1)}, ...), branch_computations={%region_0.0_spmd, %region_1.0_spmd, %region_2.0_spmd, %region_3.0_... | conditional | bytes 1704024 | solution.py:472
  78.5 0.8 branch_1_fun.2
  79.3 62.8 %all_to_all.22.rows_ref = bf16[32,48,128]{2,1,0:T(8,128)(2,1)S(1)} all-to-all(bf16[32,48,128]{2,1,0:T(8,128)(2,1)S(1)} %branch_1_fun.2), channel_id=1, replica_groups=mesh['grp'=4,'zh'=16,'zl'=2,'core'=2] {'zh','zl'}, dimensions={0} | all-to-all | bytes 786432 | tf_op jit(solution)/shard_map/cond/branch_1_fun/all_to_all | solution.py:458
  142.1 1.9 %branch_1_fun.3 = (f32[32,512]{1,0:T(8,128)S(1)}, f32[1,512]{1,0:T(1,128)S(1)}) custom-call(s32[3]{0:T(128)S(1)} %get-tuple-element.50.at_ref.took_ref, bf16[32,48,128]{2,1,0:T(8,128)(2,1)S(1)} %all_to_all.22.rows_ref, f32[64,512]{1,0:T(8,128)S(1)} %get-tuple-element.53.rank_ref, f32[64,128]{1,0:T(8,128)S(1)} %get-tuple-element.54.load_ref), custom_call_target="tpu_custom_call" | custom-call | tf_op jit(solution)/shard_map/cond/branch_1_fun/pallas_call | solution.py:459
  144.0 2.7 %collective-permute-start.6 = (f32[1,512]{1,0:T(1,128)S(1)}, f32[1,512]{1,0:T(1,128)S(1)}, u32[]{:S(2)}, u32[]{:S(2)}) collective-permute-start(f32[1,512]{1,0:T(1,128)S(1)} %get-tuple-element.81.mine_ref), channel_id=1, source_target_pairs={{0,1},{1,0},{2,3},{3,2},{4,5},{5,4},{6,7},{7,6},{8,9},{9,8},{10,11... | collective-permute-start | bytes 6152 | tf_op jit(solution)/shard_map/ppermute | solution.py:483
  146.6 0.8 collective-permute-done.6.other_ref
  147.5 25.2 %all_to_all.25.squares_ref = bf16[32,4,128]{2,1,0:T(4,128)(2,1)S(1)} all-to-all(bf16[32,4,128]{2,1,0:T(4,128)(2,1)S(1)} %shard_map.84), channel_id=1, replica_groups=mesh['grp'=4,'zh'=16,'zl'=2,'core'=2] {'zh','zl'}, dimensions={0} | all-to-all | bytes 65536 | tf_op jit(solution)/shard_map/all_to_all | solution.py:484
  172.7 0.0 copy-done
  172.7 1.4 shard_map.85
  (1 shorter events, 0.0 us)
Async XLA Ops:
  51.6 10.9 %collective-permute-start.3 = (bf16[128,2176]{1,0:T(8,128)(2,1)S(1)}, bf16[128,2176]{1,0:T(8,128)(2,1)S(1)}, u32[]{:S(2)}, u32[]{:S(2)}) collective-permute-start(bf16[128,2176]{1,0:T(8,128)(2,1)S(1)} %all_gather.3.a_ref), channel_id=1, source_target_pairs={{0,2},{1,63},{2,4},{3,1},{4,6},{5,3},{6,8},{7,5},{8,10},{9,7},{10,... | collective-permute-start | bytes 1671176 | tf_op jit(solution)/shard_map/ppermute | solution.py:396
  53.6 16.9 %collective-permute-start.2 = (bf16[128,2176]{1,0:T(8,128)(2,1)S(1)}, bf16[128,2176]{1,0:T(8,128)(2,1)S(1)}, u32[]{:S(2)}, u32[]{:S(2)}) collective-permute-start(bf16[128,2176]{1,0:T(8,128)(2,1)S(1)} %all_gather.3.a_ref), channel_id=1, source_target_pairs={{0,1},{1,0},{2,3},{3,2},{4,5},{5,4},{6,7},{7,6},{8,9},{9,8},{10,11... | collective-permute-start | bytes 1671176 | tf_op jit(solution)/shard_map/ppermute | solution.py:397
  62.5 9.5 %collective-permute-start.4 = (bf16[128,2176]{1,0:T(8,128)(2,1)S(1)}, bf16[128,2176]{1,0:T(8,128)(2,1)S(1)}, u32[]{:S(2)}, u32[]{:S(2)}) collective-permute-start(bf16[128,2176]{1,0:T(8,128)(2,1)S(1)} %collective-permute-done.3.c_ref), channel_id=1, source_target_pairs={{0,1},{1,0},{2,3},{3,2},{4,5},{5,4},{6,7},{7,6},{8,9},{9,8},{10,11... | collective-permute-start | bytes 1671176 | tf_op jit(solution)/shard_map/ppermute | solution.py:398
  76.9 1.7 collective-permute-start.5
  78.5 94.2 %copy-start = (f32[2048]{0:T(1024)S(1)}, f32[2048]{0:T(1024)}, u32[]{:S(2)}) copy-start(f32[2048]{0:T(1024)} %param.16) | copy-start | bytes 24580
  144.0 3.5 %collective-permute-start.6 = (f32[1,512]{1,0:T(1,128)S(1)}, f32[1,512]{1,0:T(1,128)S(1)}, u32[]{:S(2)}, u32[]{:S(2)}) collective-permute-start(f32[1,512]{1,0:T(1,128)S(1)} %get-tuple-element.81.mine_ref), channel_id=1, source_target_pairs={{0,1},{1,0},{2,3},{3,2},{4,5},{5,4},{6,7},{7,6},{8,9},{9,8},{10,11... | collective-permute-start | bytes 6152 | tf_op jit(solution)/shard_map/ppermute | solution.py:483
